TPU v7x, 512 devices: a whole 4x8x8 slice. The times are simulated.
512 devices in a mesh: sp: 64 (over z, y), tp: 8 (over x, core).
Axes of the slice: x: 4, y: 8, z: 8, core: 2. Of those that a mesh axis runs over, the one named last changes fastest.
Arguments:
- tokens: bfloat16 [20480, 2048], P('sp', 'tp'), may hold values from -6 to 6
- norm_gain: float32 [2048], replicated, may hold values from 0.1 to 1.9
- w_qa: bfloat16 [2048, 1024], P(None, 'tp'), may hold values from -1 to 1
- w_ka: bfloat16 [2048, 512], P(None, 'tp'), may hold values from -1 to 1
- w_va: bfloat16 [2048, 512], P(None, 'tp'), may hold values from -0.125 to 0.125
- qgain_a: float32 [16, 64], P('tp'), may hold values from 0.2 to 9
- kgain_a: float32 [8, 64], P('tp'), may hold values from 0.2 to 9
- w_qb: bfloat16 [2048, 1024], P(None, 'tp'), may hold values from -10 to 10
- w_kb: bfloat16 [2048, 512], P(None, 'tp'), may hold values from -1 to 1
- w_vb: bfloat16 [2048, 512], P(None, 'tp'), may hold values from -0.125 to 0.125
- sink_b: float32 [16], P('tp'), may hold values from 3 to 8
- w_ga: bfloat16 [2048, 1024], P(None, 'tp'), may hold values from -0.125 to 0.125
- w_gb: bfloat16 [2048, 1024], P(None, 'tp'), may hold values from -0.125 to 0.125
- out_a: bfloat16 [1024, 2048], P('tp'), may hold values from -0.375 to 0.375
- out_b: bfloat16 [1024, 2048], P('tp'), may hold values from -0.375 to 0.375
Outputs:
- mixed: bfloat16 [20480, 2048], P(('sp', 'tp'))
All inputs are finite; a program needn't handle non-finite values.
Results may differ from a plain program's by a relative error of at most 0.028.
Values may be sent and summed in bfloat16 or wider, within the bound.
No kernel may reach another device: no remote copies, remote signals or barrier semaphores. Data moves between devices by JAX's collectives and lax.ppermute only.
A program may use at most 64 MiB of HBM per device.

v0:
```python
import functools

import jax
import jax.numpy as jnp
import numpy as np
from jax import lax
from jax.experimental import pallas as pl
from jax.experimental.pallas import tpu as pltpu
from jax.sharding import Mesh, PartitionSpec as P

GRID = 64
WINDOW = 128
EPSILON = 1e-06
THETA = 10000.0
HEAD = 64
LANES = 128
BOUND = 69.0
SHIFT = 55.0
STAT_ROWS = 24
F32 = jnp.float32
BF16 = jnp.bfloat16


def rotary_tables(seq):
    quarter = HEAD // 4
    freq = np.power(np.float32(THETA), -np.arange(quarter, dtype=np.float32) / np.float32(quarter))
    freq = freq.astype(np.float32)

    def table(count, which):
        angle = (np.arange(count, dtype=np.float32)[:, None] * freq).astype(np.float64)
        out = []
        for fn in (np.cos, np.sin):
            half = np.concatenate([fn(angle), fn(angle)], axis=1)
            zero = np.zeros_like(half)
            head = np.concatenate([half, zero] if which == 0 else [zero, half], axis=1)
            out.append(np.concatenate([head, head], axis=1).astype(np.float32))
        return np.stack(out)

    return table(seq // GRID, 0), table(GRID, 1)


def dot(a, b):
    return jnp.dot(a, b, preferred_element_type=F32)


def dot_t(a, b):
    return lax.dot_general(a, b, (((1,), (1,)), ((), ())), preferred_element_type=F32)


def silu(v):
    return v / (1.0 + jnp.exp(-v))


def project_kernel(
    place_ref, mine_ref, other_ref, gain_ref, qgain_ref, kgain_ref, row_ref, col_ref,
    wqa, wka, wva, wqb, wkb, wvb, wga, wgb,
    q_out, kv_out, qb_out, kvb_out, first_out, last_out, ga_out, gb_out,
    h_s, wide_s, narrow_s, sems,
):
    wide = [wqa, wqb, wga, wgb]
    narrow = [wka, wva, wkb, wvb]
    copies = [
        pltpu.make_async_copy(ref, narrow_s.at[i * HEAD : (i + 1) * HEAD], sems.at[i])
        for i, ref in enumerate(narrow)
    ]
    copies += [
        pltpu.make_async_copy(ref, wide_s.at[i], sems.at[4 + i]) for i, ref in enumerate(wide)
    ]
    for copy in copies:
        copy.start()
    core = place_ref[0]
    s_index = place_ref[1]
    chips, rows, width = mine_ref.shape
    total = jnp.zeros((rows, 1), F32)
    for ref in (mine_ref, other_ref):
        for i in range(chips):
            part = ref[i].astype(F32)
            total = total + jnp.sum(part * part, axis=1, keepdims=True)
    scale = lax.rsqrt(total / (2 * chips * width) + EPSILON)
    for ref, side in ((mine_ref, core), (other_ref, 1 - core)):
        for i in range(chips):
            t = 2 * i + side
            h_s[t] = (ref[i].astype(F32) * scale * gain_ref[t]).astype(BF16)
    normed = jnp.concatenate([h_s[t] for t in range(2 * chips)], axis=1)
    for copy in copies:
        copy.wait()
    both_kv = dot_t(normed, narrow_s[...])
    both_q = dot(normed, jnp.concatenate([wide_s[0], wide_s[1]], axis=1))
    both_g = dot(normed, jnp.concatenate([wide_s[2], wide_s[3]], axis=1))
    ga_out[...] = both_g[:, :LANES].astype(BF16)
    gb_out[...] = both_g[:, LANES:].astype(BF16)
    qb_out[...] = both_q[:, LANES:].astype(BF16)
    kvb = both_kv[:, LANES:].astype(BF16)
    kvb_out[...] = kvb
    first_out[...] = kvb[:WINDOW]
    last_out[...] = kvb[rows - WINDOW :]
    cos = []
    sin = []
    grid_rows = rows // GRID
    for r in range(grid_rows):
        at = s_index * grid_rows + r
        cos.append(row_ref[0, pl.ds(at, 1), :] + col_ref[0])
        sin.append(row_ref[1, pl.ds(at, 1), :] + col_ref[1])
    cos = jnp.concatenate(cos, axis=0)
    sin = jnp.concatenate(sin, axis=0)
    lane = lax.broadcasted_iota(jnp.int32, (rows, LANES), 1)
    first = (lane % 32) < 16
    low = lane < HEAD

    def turned(n):
        partner = jnp.where(first, -pltpu.roll(n, LANES - 16, 1), pltpu.roll(n, 16, 1))
        return n * cos + partner * sin

    v = both_q[:, :LANES].astype(BF16).astype(F32)
    square = v * v
    sum_low = jnp.sum(jnp.where(low, square, 0.0), axis=1, keepdims=True)
    sum_high = jnp.sum(jnp.where(low, 0.0, square), axis=1, keepdims=True)
    rs_low = lax.rsqrt(sum_low / HEAD + EPSILON)
    rs_high = lax.rsqrt(sum_high / HEAD + EPSILON)
    qgain = jnp.concatenate([qgain_ref[0:1, :], qgain_ref[1:2, :]], axis=1)
    q_out[...] = turned(v * jnp.where(low, rs_low, rs_high) * qgain).astype(BF16)
    kv = both_kv[:, :LANES].astype(BF16).astype(F32)
    k_only = jnp.where(low, kv, 0.0)
    sq = jnp.sum(k_only * k_only, axis=1, keepdims=True)
    kgain = jnp.concatenate([kgain_ref[...], kgain_ref[...]], axis=1)
    ka = turned(k_only * lax.rsqrt(sq / HEAD + EPSILON) * kgain)
    both = jnp.where(low, ka, kv).astype(BF16)
    for i in range(kv_out.shape[0]):
        kv_out[i] = both


def window_kernel(
    place_ref, q_ref, mid_ref, prev_ref, next_ref, sink_ref, gate_ref, out_ref, *, count
):
    s_index = place_ref[1]
    rows = q_ref.shape[0]
    kv = jnp.concatenate([prev_ref[...], mid_ref[...], next_ref[...]], axis=0)
    span = kv.shape[0]
    r = lax.broadcasted_iota(jnp.int32, (rows, span), 0)
    c = lax.broadcasted_iota(jnp.int32, (rows, span), 1)
    place = s_index * rows - WINDOW + c
    allowed = (c >= r) & (c - r <= 2 * WINDOW) & (place >= 0) & (place < rows * count)
    q = q_ref[...] * HEAD ** (-0.5)
    stacked = jnp.concatenate([q[:, :HEAD], q[:, HEAD:]], axis=0)
    scores = dot_t(stacked, kv[:, :HEAD])
    terms = []
    dens = []
    for h in range(2):
        s = jnp.where(allowed, scores[h * rows : (h + 1) * rows], -1e30)
        sink = sink_ref[h]
        top = jnp.maximum(jnp.max(s, axis=1, keepdims=True), sink)
        p = jnp.exp(s - top)
        dens.append(jnp.sum(p, axis=1, keepdims=True) + jnp.exp(sink - top))
        terms.append(p.astype(BF16))
    mixed = dot(jnp.concatenate(terms, axis=0), kv[:, HEAD:])
    att = jnp.concatenate([mixed[:rows] / dens[0], mixed[rows:] / dens[1]], axis=1)
    out_ref[...] = (att * silu(gate_ref[...].astype(F32))).astype(BF16)


def attend_kernel(
    q_ref, kv_ref, out_ref, k_s, vt_s, qt_s, m_s, o_s, lse_s, p_s, l_s, *, tile, chunk
):
    n_q = q_ref.shape[0]
    n_k = kv_ref.shape[0]
    tiles = n_q // tile
    steps = 2 * tiles
    chunks = n_k // chunk
    kv = kv_ref[...]
    lane = lax.broadcasted_iota(jnp.int32, (n_k, LANES), 1)
    ones = jnp.where(lane < HEAD + 3, 1.0, 0.0)
    k_s[...] = jnp.where(lane < HEAD, kv.astype(F32), ones).astype(BF16)
    kv_t = kv.astype(F32).T
    k_t = kv_t[:HEAD]
    k_norm = jnp.max(jnp.sum(k_t * k_t, axis=0, keepdims=True))
    for c in range(chunks):
        vt_s[c] = kv_t[HEAD:, c * chunk : (c + 1) * chunk].astype(BF16)
    top = jnp.float32(0.0)
    for i in range(tiles):
        q_t = q_ref[i * tile : (i + 1) * tile, :].astype(F32).T
        for h in range(2):
            part = q_t[h * HEAD : (h + 1) * HEAD] * HEAD ** (-0.5)
            bound = jnp.sqrt(jnp.sum(part * part, axis=0, keepdims=True) * k_norm) * 1.0001
            top = jnp.maximum(top, jnp.max(bound))
            m_s[2 * i + h] = bound - SHIFT
            qt_s[2 * i + h, :HEAD] = part.astype(BF16)
            qt_s[2 * i + h, HEAD:] = jnp.zeros((LANES - HEAD, tile), BF16)

    @pl.when(top > BOUND)
    def _():
        def row_max(t, carry):
            def one(c, m):
                s = dot(k_s[pl.ds(pl.multiple_of(c * chunk, chunk), chunk), :], qt_s[t])
                return jnp.maximum(m, jnp.max(s, axis=0, keepdims=True))

            m_s[t] = lax.fori_loop(0, chunks, one, jnp.full((1, tile), -1e30, F32))
            return carry

        lax.fori_loop(0, steps, row_max, 0)

    row = lax.broadcasted_iota(jnp.int32, (16, tile), 0)
    for t in range(steps):
        neg = -m_s[t]
        hi = neg.astype(BF16).astype(F32)
        mid = (neg - hi).astype(BF16).astype(F32)
        lo = neg - hi - mid
        parts = jnp.where(row == 0, hi, jnp.where(row == 1, mid, jnp.where(row == 2, lo, 0.0)))
        qt_s[t, HEAD : HEAD + 16] = parts.astype(BF16)

    def both(ahead, ahead_slot, now, now_slot):
        if ahead is not None:
            q_here = qt_s[ahead]
            sums = jnp.zeros((8, tile), F32)
        acc = jnp.zeros((HEAD, tile), F32)
        for c in range(chunks):
            if ahead is not None:
                e = jnp.exp(dot(k_s[c * chunk : (c + 1) * chunk, :], q_here))
                sums = sums + jnp.sum(e.reshape(chunk // 8, 8, tile), axis=0)
                p_s[ahead_slot, c] = e.astype(BF16)
            if now is not None:
                acc = acc + dot(vt_s[c], p_s[now_slot, c])
        if now is not None:
            total = jnp.sum(l_s[now_slot], axis=0, keepdims=True)
            lse_s[now] = m_s[now] + jnp.log(total)
            o_s[now] = acc / total
        if ahead is not None:
            l_s[ahead_slot] = sums

    both(0, 0, None, None)

    def pair(n, carry):
        both(2 * n + 1, 1, 2 * n, 0)
        both(2 * n + 2, 0, 2 * n + 1, 1)
        return carry

    lax.fori_loop(0, (steps - 2) // 2, pair, 0)
    both(steps - 1, 1, steps - 2, 0)
    both(None, None, steps - 1, 1)

    lse = jnp.concatenate(
        [jnp.concatenate([lse_s[2 * i], lse_s[2 * i + 1]], axis=0) for i in range(tiles)], axis=1
    )
    hi = lse.astype(BF16).astype(F32)
    mid = (lse - hi).astype(BF16).astype(F32)
    lo = lse - hi - mid
    stats = jnp.concatenate([hi, mid, lo, jnp.zeros_like(hi)], axis=0)
    stats = jnp.concatenate([stats, jnp.zeros((8, LANES), F32)], axis=1)
    blocks = out_ref.shape[0]
    rows = n_q // blocks
    flat = jnp.concatenate(
        [
            jnp.concatenate([o_s[2 * i], o_s[2 * i + 1]], axis=0).T.astype(BF16)
            for i in range(tiles)
        ],
        axis=0,
    )
    for b in range(blocks):
        out_ref[b, :rows] = flat[b * rows : (b + 1) * rows]
        for k in range(STAT_ROWS // 8):
            at = b * rows + k * LANES
            out_ref[b, rows + 8 * k : rows + 8 * k + 8] = stats[:, at : at + LANES].astype(BF16)


def combine_kernel(
    place_ref, part_ref, ga_ref, gated_b_ref, wa_ref, wb_ref, kept_ref, sent_ref, out_s
):
    blocks, padded, _ = part_ref.shape
    rows = padded - STAT_ROWS
    lses = []
    for s in range(blocks):
        pieces = [
            part_ref[s, rows + 8 * k : rows + 8 * k + 8].astype(F32) for k in range(STAT_ROWS // 8)
        ]
        x = jnp.concatenate(pieces, axis=1)
        lses.append(x[0:2] + x[2:4] + x[4:6])
    top = functools.reduce(jnp.maximum, lses)
    weights = [jnp.exp(v - top) for v in lses]
    den = functools.reduce(jnp.add, weights)
    stacked = jnp.concatenate([v / den for v in weights], axis=0)
    cols = jnp.concatenate(
        [stacked, jnp.zeros((LANES - 2 * blocks, stacked.shape[1]), F32)], axis=0
    ).T
    low = lax.broadcasted_iota(jnp.int32, (rows, LANES), 1) < HEAD
    acc = jnp.zeros((rows, LANES), F32)
    for s in range(blocks):
        w = jnp.where(low, cols[:rows, 2 * s : 2 * s + 1], cols[:rows, 2 * s + 1 : 2 * s + 2])
        acc = acc + w * part_ref[s, :rows].astype(F32)
    gated_a = (acc * silu(ga_ref[...].astype(F32))).astype(BF16)
    gated = jnp.concatenate([gated_a, gated_b_ref[...]], axis=1)
    w = jnp.concatenate([wa_ref[...], wb_ref[...]], axis=0)
    result = dot(gated, w).astype(BF16)
    core = place_ref[0]
    chips, piece, _ = kept_ref.shape
    for t in range(2 * chips):
        out_s[t] = result[t * piece : (t + 1) * piece]
    for i in range(chips):
        kept_ref[i] = out_s[2 * i + core]
        sent_ref[i] = out_s[2 * i + 1 - core]


def call(kernel, outs, scratch, smem, near, *args, name, flops=0, far=()):
    args = [
        pltpu.with_memory_space_constraint(a, pltpu.VMEM) if i in near else a
        for i, a in enumerate(args)
    ]
    specs = [
        pl.BlockSpec(
            memory_space=pltpu.SMEM if i in smem else pl.ANY if i in far else pltpu.VMEM
        )
        for i in range(len(args))
    ]
    return pl.pallas_call(
        kernel,
        out_shape=outs,
        in_specs=specs,
        out_specs=(
            tuple(pl.BlockSpec(memory_space=pltpu.VMEM) for _ in outs)
            if isinstance(outs, tuple)
            else pl.BlockSpec(memory_space=pltpu.VMEM)
        ),
        scratch_shapes=scratch,
        compiler_params=pltpu.CompilerParams(vmem_limit_bytes=56 * 2**20),
        cost_estimate=pl.CostEstimate(flops=flops, bytes_accessed=2**20, transcendentals=0),
        name=name,
    )(*args)


def shaped(*shape, dtype=BF16):
    return pltpu.VMEM(shape, dtype)


def body(
    tokens, norm_gain, w_qa, w_ka, w_va, qgain_a, kgain_a, w_qb, w_kb, w_vb, sink_b, w_ga, w_gb,
    out_a, out_b,
):
    rows, width = tokens.shape
    n_z, n_y, n_x = (lax.axis_size(a) for a in ("z", "y", "x"))
    blocks = n_z * n_y
    tp = 2 * n_x
    s_index = lax.axis_index("z") * n_y + lax.axis_index("y")
    core = lax.axis_index("core")
    place = jnp.stack([core, s_index]).astype(jnp.int32)
    row_table, col_table = rotary_tables(blocks * rows)

    mine = lax.all_gather(tokens, "x", axis=0)
    other = lax.ppermute(mine, "core", [(0, 1), (1, 0)])
    q, kv8, qb, kvb, kvb_first, kvb_last, ga, gb = call(
        project_kernel,
        (
            shaped(rows, LANES), shaped(n_z, rows, LANES),
            shaped(rows, LANES), shaped(rows, LANES),
            shaped(WINDOW, LANES), shaped(WINDOW, LANES),
            shaped(rows, LANES), shaped(rows, LANES),
        ),
        [
            pltpu.VMEM((tp, rows, width), BF16),
            pltpu.VMEM((4, tp * width, LANES), BF16),
            pltpu.VMEM((4 * HEAD, tp * width), BF16),
            pltpu.SemaphoreType.DMA((8,)),
        ],
        {0},
        {1, 2},
        place, mine, other, norm_gain.reshape(tp, 1, width), qgain_a, kgain_a,
        jnp.asarray(row_table), jnp.asarray(col_table),
        w_qa, w_ka.T, w_va.T, w_qb, w_kb.T, w_vb.T, w_ga, w_gb,
        name="project", flops=2 * rows * width * tp * 768, far=set(range(8, 16)),
    )
    kv_all = lax.all_to_all(kv8, "z", 0, 0, tiled=True)
    q_all = lax.all_gather(q, "y", axis=0, tiled=True)
    up = [(i, i + 1) for i in range(blocks - 1)]
    down = [(i + 1, i) for i in range(blocks - 1)]
    before = lax.ppermute(kvb_last, ("z", "y"), up)
    after = lax.ppermute(kvb_first, ("z", "y"), down)
    gated_b = call(
        functools.partial(window_kernel, count=blocks),
        shaped(rows, LANES),
        [],
        {0, 5},
        {1, 2, 3, 4, 6},
        place, qb, kvb, before, after, sink_b, gb,
        name="windowed", flops=4 * 2 * rows * 576 * 64,
    )
    n_q = n_y * rows
    n_k = n_z * rows
    tile = 512
    chunk = 256
    steps = 2 * n_q // tile
    parts = call(
        functools.partial(attend_kernel, tile=tile, chunk=chunk),
        shaped(n_y, rows + STAT_ROWS, LANES),
        [
            pltpu.VMEM((n_k, LANES), BF16),
            pltpu.VMEM((n_k // chunk, HEAD, chunk), BF16),
            pltpu.VMEM((steps, LANES, tile), BF16),
            pltpu.VMEM((steps, 1, tile), F32),
            pltpu.VMEM((steps, HEAD, tile), F32),
            pltpu.VMEM((steps, 1, tile), F32),
            pltpu.VMEM((2, n_k // chunk, chunk, tile), BF16),
            pltpu.VMEM((2, 8, tile), F32),
        ],
        {},
        {0, 1},
        q_all, kv_all.reshape(n_k, LANES),
        name="attend", flops=4 * 2 * n_q * n_k * 64,
    )
    back = lax.all_to_all(parts, "y", 0, 0, tiled=True)
    piece = shaped(n_x, rows // tp, out_a.shape[1])
    kept, sent = call(
        combine_kernel,
        (piece, piece),
        [pltpu.VMEM((tp, rows // tp, out_a.shape[1]), BF16)],
        {0},
        {1, 2, 3, 4, 5},
        place, back, ga, gated_b, out_a, out_b,
        name="combine", flops=2 * rows * 256 * 2048,
    )
    got = lax.ppermute(sent, "core", [(0, 1), (1, 0)])
    paired = (kept.astype(F32) + got.astype(F32)).astype(BF16)
    arrived = lax.all_to_all(paired, "x", 0, 0, tiled=True)
    return jnp.sum(arrived.astype(F32), axis=0).astype(BF16)


def solution(mesh):
    n_sp, n_tp = (mesh.shape["sp"], mesh.shape["tp"])
    n_z = 8
    fine = Mesh(
        np.asarray(mesh.devices).reshape(n_z, n_sp // n_z, n_tp // 2, 2), ("z", "y", "x", "core")
    )
    sp = ("z", "y")
    tp = ("x", "core")
    placed = (
        P(sp, tp), P(), P(None, tp), P(None, tp), P(None, tp), P(tp, None), P(tp, None),
        P(None, tp), P(None, tp), P(None, tp), P(tp), P(None, tp), P(None, tp), P(tp, None),
        P(tp, None),
    )
    return jax.shard_map(
        body, mesh=fine, in_specs=placed, out_specs=P((*sp, *tp), None), check_vma=False
    )
```

profile of v0, /device:TPU:1, one launch (start us, length us, event | category | flops | bytes accessed | tf_op | source)
XLA Modules:
  0.0 137.1 jit_solution(4044133090119110745)
XLA Ops:
  0.0 11.5 %all-gather = bf16[1280,256]{1,0:T(8,128)(2,1)S(1)} all-gather(bf16[320,256]{1,0:T(8,128)(2,1)} %param.17), channel_id=2, replica_groups=mesh['z'=8,'y'=8,'x'=4,'core'=2] {'x'}, dimensions={0}, use_global_device_ids=true | all-gather | bytes 819200 | tf_op jit(solution)/shard_map/all_gather | solution.py:344
  11.5 10.5 %collective-permute-start = (bf16[4,320,256]{2,1,0:T(8,128)(2,1)S(1)}, bf16[4,320,256]{2,1,0:T(8,128)(2,1)S(1)}, u32[]{:S(2)}, u32[]{:S(2)}) collective-permute-start(bf16[4,320,256]{2,1,0:T(8,128)(2,1)S(1)} %bitcast.9), channel_id=1, source_target_pairs={{0,1},{1,0},{2,3},{3,2},{4,5},{5,4},{6,7},{7,6},{8,9},{9,8},{10,11... | collective-permute-start | bytes 1966088 | tf_op jit(solution)/shard_map/ppermute | solution.py:345
  22.0 0.6 pad_add_fusion.place_ref
  22.6 1.1 collective-permute-done.other_ref
  23.7 5.7 %project.1 = (bf16[320,128]{1,0:T(8,128)(2,1)S(1)}, bf16[8,320,128]{2,1,0:T(8,128)(2,1)}, bf16[320,128]{1,0:T(8,128)(2,1)S(1)}, bf16[320,128]{1,0:T(8,128)(2,1)S...) custom-call(s32[2]{0:T(128)} %pad_add_fusion.place_ref, ...), custom_call_target="tpu_custom_call" | custom-call | flops 1006632960 | bytes 1048576 | tf_op jit(solution)/shard_map/project/pallas_call | solution.py:311
  29.4 5.1 %all-to-all-start = ((bf16[8,320,128]{2,1,0:T(8,128)(2,1)}), bf16[8,320,128]{2,1,0:T(8,128)(2,1)S(1)}, u32[]{:S(2)}, u32[]{:S(2)}) async-start(bf16[8,320,128]{2,1,0:T(8,128)(2,1)} %get-tuple-element.16), calls=%async_computation | async-start | bytes 1310720 | tf_op jit(solution)/shard_map/all_to_all | solution.py:367
  34.5 22.1 %all_gather.11.q_ref = bf16[2560,128]{1,0:T(8,128)(2,1)S(1)} all-gather(bf16[320,128]{1,0:T(8,128)(2,1)S(1)} %get-tuple-element.15), channel_id=1, replica_groups=mesh['z'=8,'y'=8,'x'=4,'core'=2] {'y'}, dimensions={0}, use_global_device_ids=true | all-gather | bytes 737280 | tf_op jit(solution)/shard_map/all_gather | solution.py:368
  56.5 0.0 all-to-all-done
  56.5 12.0 %attend.1 = bf16[8,344,128]{2,1,0:T(8,128)(2,1)} custom-call(bf16[2560,128]{1,0:T(8,128)(2,1)S(1)} %all_gather.11.q_ref, bf16[2560,128]{1,0:T(8,128)(2,1)S(1)} %bitcast.11), custom_call_target="tpu_custom_call" | custom-call | flops 3355443200 | bytes 1048576 | tf_op jit(solution)/shard_map/attend/pallas_call | solution.py:311
  68.5 5.8 %all-to-all-start.1 = ((bf16[8,344,128]{2,1,0:T(8,128)(2,1)}), bf16[8,344,128]{2,1,0:T(8,128)(2,1)S(1)}, u32[]{:S(2)}, u32[]{:S(2)}) async-start(bf16[8,344,128]{2,1,0:T(8,128)(2,1)} %attend.1), calls=%async_computation.1 | async-start | bytes 1409024 | tf_op jit(solution)/shard_map/all_to_all | solution.py:405
  74.3 3.4 %collective-permute-start.1 = (bf16[128,128]{1,0:T(8,128)(2,1)S(1)}, bf16[128,128]{1,0:T(8,128)(2,1)S(1)}, u32[]{:S(2)}, u32[]{:S(2)}) collective-permute-start(bf16[128,128]{1,0:T(8,128)(2,1)S(1)} %get-tuple-element.20), channel_id=1, source_target_pairs={{0,8},{8,16},{16,24},{24,32},{32,40},{40,48},{48,56},{56,64},{64,7... | collective-permute-start | bytes 98312 | tf_op jit(solution)/shard_map/ppermute | solution.py:371
  77.6 1.3 collective-permute-start.2
  78.9 3.1 %collective-permute-done.1.prev_ref = bf16[128,128]{1,0:T(8,128)(2,1)S(1)} collective-permute-done((bf16[128,128]{1,0:T(8,128)(2,1)S(1)}, bf16[128,128]{1,0:T(8,128)(2,1)S(1)}, u32[]{:S(2)}, u32[]{:S(2)}) %collective-permute-start.1) | collective-permute-done | bytes 32800 | tf_op jit(solution)/shard_map/ppermute | solution.py:371
  82.1 4.9 %collective-permute-done.2.next_ref = bf16[128,128]{1,0:T(8,128)(2,1)S(1)} collective-permute-done((bf16[128,128]{1,0:T(8,128)(2,1)S(1)}, bf16[128,128]{1,0:T(8,128)(2,1)S(1)}, u32[]{:S(2)}, u32[]{:S(2)}) %collective-permute-start.2) | collective-permute-done | bytes 32800 | tf_op jit(solution)/shard_map/ppermute | solution.py:372
  86.9 1.8 %windowed.1.gated_b_ref = bf16[320,128]{1,0:T(8,128)(2,1)S(1)} custom-call(s32[2]{0:T(128)} %pad_add_fusion.place_ref, bf16[320,128]{1,0:T(8,128)(2,1)S(1)} %get-tuple-element.18.q_ref, bf16[320,128]{1,0:T(8,128)(2,1)S(1)} %get-tuple-element.19.mid_ref, bf16[128,128]{1,0:T(8,128)(2,1)S(1)} %collective-permute-done.1.prev_ref, ...), custom_call_target="tpu_custom_call" | custom-call | flops 94371840 | bytes 1048576 | tf_op jit(solution)/shard_map/windowed/pallas_call | solution.py:311
  88.7 0.0 all-to-all-done.1.part_ref
  88.7 0.0 copy-done
  88.7 0.0 copy-done.1
  88.7 2.2 %combine.1 = (bf16[4,40,2048]{2,1,0:T(8,128)(2,1)S(1)}, bf16[4,40,2048]{2,1,0:T(8,128)(2,1)S(1)}) custom-call(s32[2]{0:T(128)} %pad_add_fusion.place_ref, bf16[8,344,128]{2,1,0:T(8,128)(2,1)S(1)} %all-to-all-done.1.part_ref, bf16[320,128]{1,0:T(8,128)(2,1)S(1)} %get-tuple-element.17.ga_ref, bf16[320,128]{1,0:T(8,128)(2,1)S(1)} %windowed.1.gated_b_ref, ...), custom_call_target="tpu_custom_call" | custom-call | flops 335544320 | bytes 1048576 | tf_op jit(solution)/shard_map/combine/pallas_call | solution.py:311
  91.0 10.2 %collective-permute-start.3 = (bf16[4,40,2048]{2,1,0:T(8,128)(2,1)S(1)}, bf16[4,40,2048]{2,1,0:T(8,128)(2,1)S(1)}, u32[]{:S(2)}, u32[]{:S(2)}) collective-permute-start(bf16[4,40,2048]{2,1,0:T(8,128)(2,1)S(1)} %get-tuple-element.24), channel_id=1, source_target_pairs={{0,1},{1,0},{2,3},{3,2},{4,5},{5,4},{6,7},{7,6},{8,9},{9,8},{10,11... | collective-permute-start | bytes 1966088 | tf_op jit(solution)/shard_map/ppermute | solution.py:416
  101.1 1.7 %collective-permute-done.3 = bf16[4,40,2048]{2,1,0:T(8,128)(2,1)S(1)} collective-permute-done((bf16[4,40,2048]{2,1,0:T(8,128)(2,1)S(1)}, bf16[4,40,2048]{2,1,0:T(8,128)(2,1)S(1)}, u32[]{:S(2)}, u32[]{:S(2)}) %collective-permute-start.3) | collective-permute-done | bytes 655392 | tf_op jit(solution)/shard_map/ppermute | solution.py:416
  102.8 0.2 add_convert_fusion
  103.1 33.3 %all_to_all.15 = bf16[4,40,2048]{2,1,0:T(8,128)(2,1)S(1)} all-to-all(bf16[4,40,2048]{2,1,0:T(8,128)(2,1)S(1)} %add_convert_fusion), channel_id=1, replica_groups=mesh['z'=8,'y'=8,'x'=4,'core'=2] {'x'}, dimensions={0} | all-to-all | bytes 1310720 | tf_op jit(solution)/shard_map/all_to_all | solution.py:418
  136.4 0.8 reduce_sum.12
  (2 shorter events, 0.0 us)
Async XLA Ops:
  11.5 12.2 %collective-permute-start = (bf16[4,320,256]{2,1,0:T(8,128)(2,1)S(1)}, bf16[4,320,256]{2,1,0:T(8,128)(2,1)S(1)}, u32[]{:S(2)}, u32[]{:S(2)}) collective-permute-start(bf16[4,320,256]{2,1,0:T(8,128)(2,1)S(1)} %bitcast.9), channel_id=1, source_target_pairs={{0,1},{1,0},{2,3},{3,2},{4,5},{5,4},{6,7},{7,6},{8,9},{9,8},{10,11... | collective-permute-start | bytes 1966088 | tf_op jit(solution)/shard_map/ppermute | solution.py:345
  29.4 27.1 %all-to-all-start = ((bf16[8,320,128]{2,1,0:T(8,128)(2,1)}), bf16[8,320,128]{2,1,0:T(8,128)(2,1)S(1)}, u32[]{:S(2)}, u32[]{:S(2)}) async-start(bf16[8,320,128]{2,1,0:T(8,128)(2,1)} %get-tuple-element.16), calls=%async_computation | async-start | bytes 1310720 | tf_op jit(solution)/shard_map/all_to_all | solution.py:367
  68.5 20.2 %copy-start = (bf16[128,2048]{1,0:T(8,128)(2,1)S(1)}, bf16[128,2048]{1,0:T(8,128)(2,1)}, u32[]{:S(2)}) copy-start(bf16[128,2048]{1,0:T(8,128)(2,1)} %wa_ref.1) | copy-start | bytes 1572868
  68.5 20.2 %copy-start.1 = (bf16[128,2048]{1,0:T(8,128)(2,1)S(1)}, bf16[128,2048]{1,0:T(8,128)(2,1)}, u32[]{:S(2)}) copy-start(bf16[128,2048]{1,0:T(8,128)(2,1)} %wb_ref.1) | copy-start | bytes 1572868
  68.5 20.2 %all-to-all-start.1 = ((bf16[8,344,128]{2,1,0:T(8,128)(2,1)}), bf16[8,344,128]{2,1,0:T(8,128)(2,1)S(1)}, u32[]{:S(2)}, u32[]{:S(2)}) async-start(bf16[8,344,128]{2,1,0:T(8,128)(2,1)} %attend.1), calls=%async_computation.1 | async-start | bytes 1409024 | tf_op jit(solution)/shard_map/all_to_all | solution.py:405
  74.3 7.8 %collective-permute-start.1 = (bf16[128,128]{1,0:T(8,128)(2,1)S(1)}, bf16[128,128]{1,0:T(8,128)(2,1)S(1)}, u32[]{:S(2)}, u32[]{:S(2)}) collective-permute-start(bf16[128,128]{1,0:T(8,128)(2,1)S(1)} %get-tuple-element.20), channel_id=1, source_target_pairs={{0,8},{8,16},{16,24},{24,32},{32,40},{40,48},{48,56},{56,64},{64,7... | collective-permute-start | bytes 98312 | tf_op jit(solution)/shard_map/ppermute | solution.py:371
  77.6 9.3 %collective-permute-start.2 = (bf16[128,128]{1,0:T(8,128)(2,1)S(1)}, bf16[128,128]{1,0:T(8,128)(2,1)S(1)}, u32[]{:S(2)}, u32[]{:S(2)}) collective-permute-start(bf16[128,128]{1,0:T(8,128)(2,1)S(1)} %get-tuple-element.21), channel_id=1, source_target_pairs={{8,0},{16,8},{24,16},{32,24},{40,32},{48,40},{56,48},{64,56},{72,6... | collective-permute-start | bytes 98312 | tf_op jit(solution)/shard_map/ppermute | solution.py:372
  91.0 11.9 %collective-permute-start.3 = (bf16[4,40,2048]{2,1,0:T(8,128)(2,1)S(1)}, bf16[4,40,2048]{2,1,0:T(8,128)(2,1)S(1)}, u32[]{:S(2)}, u32[]{:S(2)}) collective-permute-start(bf16[4,40,2048]{2,1,0:T(8,128)(2,1)S(1)} %get-tuple-element.24), channel_id=1, source_target_pairs={{0,1},{1,0},{2,3},{3,2},{4,5},{5,4},{6,7},{7,6},{8,9},{9,8},{10,11... | collective-permute-start | bytes 1966088 | tf_op jit(solution)/shard_map/ppermute | solution.py:416
where the time goes:
time: 135 us; the launch traced here: 137 us
  blocking collectives  66.9 us (50%)
  starting transfers between devices  36.1 us (27%)
  Pallas kernels  21.7 us (16%)
  waiting for transfers between devices  10.7 us (8%)
  other arithmetic  1.62 us (1%)
    all_to_all x1, blocking collectives, body(): arrived = lax.all_to_all(paired, 'x', 0, 0, tiled=True)  33.3 us
    all_gather x1, blocking collectives, body(): q_all = lax.all_gather(q, 'y', axis=0, tiled=True)  22.1 us
    pallas_call x4, Pallas kernels, call(): pl.pallas_call(kernel, out_shape=outs, in_specs=specs, out_specs=tuple((p...  21.7 us
    all_gather x1, blocking collectives, body(): mine = lax.all_gather(tokens, 'x', axis=0)  11.5 us
    ppermute x1, starting transfers between devices, body(): other = lax.ppermute(mine, 'core', [(0, 1), (1, 0)])  10.5 us
    ppermute x1, starting transfers between devices, body(): got = lax.ppermute(sent, 'core', [(0, 1), (1, 0)])  10.2 us
    all_to_all x1, starting transfers between devices, body(): back = lax.all_to_all(parts, 'y', 0, 0, tiled=True)  5.76 us
    all_to_all x1, starting transfers between devices, body(): kv_all = lax.all_to_all(kv8, 'z', 0, 0, tiled=True)  5.05 us
  transfers between devices with their start and end apart: 6, of which 4 were waited for; matrix products, arithmetic and copies ran while one was open for 0% of the time, Pallas kernels for 1%

commit v1 on v0

--- a/solution.py
+++ b/solution.py
@@ -21,7 +21,7 @@
 BF16 = jnp.bfloat16
 
 
-def rotary_tables(seq):
+def rotary_tables(seq, blocks):
     quarter = HEAD // 4
     freq = np.power(np.float32(THETA), -np.arange(quarter, dtype=np.float32) / np.float32(quarter))
     freq = freq.astype(np.float32)
@@ -36,7 +36,11 @@
             out.append(np.concatenate([head, head], axis=1).astype(np.float32))
         return np.stack(out)
 
-    return table(seq // GRID, 0), table(GRID, 1)
+    by_row = table(seq // GRID, 0).reshape(2, blocks, -1, LANES)
+    padded = np.zeros((blocks, 16, LANES), np.float32)
+    padded[:, : by_row.shape[2]] = by_row[0]
+    padded[:, 8 : 8 + by_row.shape[2]] = by_row[1]
+    return padded, table(GRID, 1)
 
 
 def dot(a, b):
@@ -52,14 +56,16 @@
 
 
 def project_kernel(
-    place_ref, mine_ref, other_ref, gain_ref, qgain_ref, kgain_ref, row_ref, col_ref,
-    wqa, wka, wva, wqb, wkb, wvb, wga, wgb,
-    q_out, kv_out, qb_out, kvb_out, first_out, last_out, ga_out, gb_out,
-    h_s, wide_s, narrow_s, sems,
+    place_ref, mine_ref, other_ref, gain_ref, qgain_ref, kgain_ref, col_ref, row_ref,
+    wqa, wka, wva, wqb, wkb, wvb,
+    q_out, kv_out, qb_out, kvb_out, first_out, last_out, h_out,
+    h_s, wide_s, narrow_s, row_s, sems,
 ):
-    wide = [wqa, wqb, wga, wgb]
+    core = place_ref[0]
+    wide = [wqa, wqb]
     narrow = [wka, wva, wkb, wvb]
-    copies = [
+    copies = [pltpu.make_async_copy(row_ref.at[place_ref[1]], row_s, sems.at[6])]
+    copies += [
         pltpu.make_async_copy(ref, narrow_s.at[i * HEAD : (i + 1) * HEAD], sems.at[i])
         for i, ref in enumerate(narrow)
     ]
@@ -68,41 +74,36 @@
     ]
     for copy in copies:
         copy.start()
-    core = place_ref[0]
-    s_index = place_ref[1]
     chips, rows, width = mine_ref.shape
-    total = jnp.zeros((rows, 1), F32)
-    for ref in (mine_ref, other_ref):
-        for i in range(chips):
-            part = ref[i].astype(F32)
-            total = total + jnp.sum(part * part, axis=1, keepdims=True)
-    scale = lax.rsqrt(total / (2 * chips * width) + EPSILON)
-    for ref, side in ((mine_ref, core), (other_ref, 1 - core)):
-        for i in range(chips):
-            t = 2 * i + side
-            h_s[t] = (ref[i].astype(F32) * scale * gain_ref[t]).astype(BF16)
-    normed = jnp.concatenate([h_s[t] for t in range(2 * chips)], axis=1)
+    count = 2 * chips
+    block = GRID
+
+    def normalise(r, carry):
+        at = pl.ds(pl.multiple_of(r * block, block), block)
+        parts = [ref[i, at, :].astype(F32) for ref in (mine_ref, other_ref) for i in range(chips)]
+        squares = functools.reduce(jnp.add, [v * v for v in parts])
+        total = jnp.sum(squares, axis=1, keepdims=True)
+        scale = lax.rsqrt(total / (count * width) + EPSILON)
+        for n, v in enumerate(parts):
+            t = 2 * (n % chips) + (core if n < chips else 1 - core)
+            h_s[t, at, :] = (v * scale * gain_ref[t]).astype(BF16)
+        return carry
+
+    lax.fori_loop(0, rows // block, normalise, 0)
+    normed = jnp.concatenate([h_s[t] for t in range(count)], axis=1)
+    h_out[...] = normed
     for copy in copies:
         copy.wait()
     both_kv = dot_t(normed, narrow_s[...])
     both_q = dot(normed, jnp.concatenate([wide_s[0], wide_s[1]], axis=1))
-    both_g = dot(normed, jnp.concatenate([wide_s[2], wide_s[3]], axis=1))
-    ga_out[...] = both_g[:, :LANES].astype(BF16)
-    gb_out[...] = both_g[:, LANES:].astype(BF16)
     qb_out[...] = both_q[:, LANES:].astype(BF16)
     kvb = both_kv[:, LANES:].astype(BF16)
     kvb_out[...] = kvb
     first_out[...] = kvb[:WINDOW]
     last_out[...] = kvb[rows - WINDOW :]
-    cos = []
-    sin = []
     grid_rows = rows // GRID
-    for r in range(grid_rows):
-        at = s_index * grid_rows + r
-        cos.append(row_ref[0, pl.ds(at, 1), :] + col_ref[0])
-        sin.append(row_ref[1, pl.ds(at, 1), :] + col_ref[1])
-    cos = jnp.concatenate(cos, axis=0)
-    sin = jnp.concatenate(sin, axis=0)
+    cos = jnp.concatenate([row_s[r : r + 1] + col_ref[0] for r in range(grid_rows)], axis=0)
+    sin = jnp.concatenate([row_s[8 + r : 9 + r] + col_ref[1] for r in range(grid_rows)], axis=0)
     lane = lax.broadcasted_iota(jnp.int32, (rows, LANES), 1)
     first = (lane % 32) < 16
     low = lane < HEAD
@@ -118,15 +119,22 @@
     rs_low = lax.rsqrt(sum_low / HEAD + EPSILON)
     rs_high = lax.rsqrt(sum_high / HEAD + EPSILON)
     qgain = jnp.concatenate([qgain_ref[0:1, :], qgain_ref[1:2, :]], axis=1)
-    q_out[...] = turned(v * jnp.where(low, rs_low, rs_high) * qgain).astype(BF16)
+    qa = turned(v * jnp.where(low, rs_low, rs_high) * qgain).astype(BF16)
+    for i in range(q_out.shape[0]):
+        q_out[i] = qa
     kv = both_kv[:, :LANES].astype(BF16).astype(F32)
     k_only = jnp.where(low, kv, 0.0)
     sq = jnp.sum(k_only * k_only, axis=1, keepdims=True)
     kgain = jnp.concatenate([kgain_ref[...], kgain_ref[...]], axis=1)
     ka = turned(k_only * lax.rsqrt(sq / HEAD + EPSILON) * kgain)
-    both = jnp.where(low, ka, kv).astype(BF16)
-    for i in range(kv_out.shape[0]):
-        kv_out[i] = both
+    kv_out[...] = jnp.where(low, ka, kv).astype(BF16)
+
+
+def gate_kernel(h_ref, wa_ref, wb_ref, ga_out, gb_out):
+    both = dot(h_ref[...], jnp.concatenate([wa_ref[...], wb_ref[...]], axis=1))
+    gates = silu(both.astype(BF16).astype(F32))
+    ga_out[...] = gates[:, :LANES]
+    gb_out[...] = gates[:, LANES:]
 
 
 def window_kernel(
@@ -154,7 +162,7 @@
         terms.append(p.astype(BF16))
     mixed = dot(jnp.concatenate(terms, axis=0), kv[:, HEAD:])
     att = jnp.concatenate([mixed[:rows] / dens[0], mixed[rows:] / dens[1]], axis=1)
-    out_ref[...] = (att * silu(gate_ref[...].astype(F32))).astype(BF16)
+    out_ref[...] = (att * gate_ref[...]).astype(BF16)
 
 
 def attend_kernel(
@@ -284,7 +292,7 @@
     for s in range(blocks):
         w = jnp.where(low, cols[:rows, 2 * s : 2 * s + 1], cols[:rows, 2 * s + 1 : 2 * s + 2])
         acc = acc + w * part_ref[s, :rows].astype(F32)
-    gated_a = (acc * silu(ga_ref[...].astype(F32))).astype(BF16)
+    gated_a = (acc * ga_ref[...]).astype(BF16)
     gated = jnp.concatenate([gated_a, gated_b_ref[...]], axis=1)
     w = jnp.concatenate([wa_ref[...], wb_ref[...]], axis=0)
     result = dot(gated, w).astype(BF16)
@@ -339,54 +347,46 @@
     s_index = lax.axis_index("z") * n_y + lax.axis_index("y")
     core = lax.axis_index("core")
     place = jnp.stack([core, s_index]).astype(jnp.int32)
-    row_table, col_table = rotary_tables(blocks * rows)
+    row_table, col_table = rotary_tables(blocks * rows, blocks)
 
     mine = lax.all_gather(tokens, "x", axis=0)
     other = lax.ppermute(mine, "core", [(0, 1), (1, 0)])
-    q, kv8, qb, kvb, kvb_first, kvb_last, ga, gb = call(
+    q8, kv, qb, kvb, kvb_first, kvb_last, normed = call(
         project_kernel,
         (
-            shaped(rows, LANES), shaped(n_z, rows, LANES),
+            shaped(n_z, rows, LANES), shaped(rows, LANES),
             shaped(rows, LANES), shaped(rows, LANES),
             shaped(WINDOW, LANES), shaped(WINDOW, LANES),
-            shaped(rows, LANES), shaped(rows, LANES),
+            shaped(rows, tp * width),
         ),
         [
             pltpu.VMEM((tp, rows, width), BF16),
-            pltpu.VMEM((4, tp * width, LANES), BF16),
+            pltpu.VMEM((2, tp * width, LANES), BF16),
             pltpu.VMEM((4 * HEAD, tp * width), BF16),
-            pltpu.SemaphoreType.DMA((8,)),
+            pltpu.VMEM((16, LANES), F32),
+            pltpu.SemaphoreType.DMA((7,)),
         ],
         {0},
         {1, 2},
         place, mine, other, norm_gain.reshape(tp, 1, width), qgain_a, kgain_a,
-        jnp.asarray(row_table), jnp.asarray(col_table),
-        w_qa, w_ka.T, w_va.T, w_qb, w_kb.T, w_vb.T, w_ga, w_gb,
-        name="project", flops=2 * rows * width * tp * 768, far=set(range(8, 16)),
-    )
-    kv_all = lax.all_to_all(kv8, "z", 0, 0, tiled=True)
-    q_all = lax.all_gather(q, "y", axis=0, tiled=True)
+        jnp.asarray(col_table), jnp.asarray(row_table),
+        w_qa, w_ka.T, w_va.T, w_qb, w_kb.T, w_vb.T,
+        name="project", flops=2 * rows * width * tp * 512, far=set(range(7, 14)),
+    )
+    q_all = lax.all_to_all(q8, "z", 0, 0, tiled=True)
+    kv_all = lax.all_gather(kv, "y", axis=0, tiled=True)
     up = [(i, i + 1) for i in range(blocks - 1)]
     down = [(i + 1, i) for i in range(blocks - 1)]
     before = lax.ppermute(kvb_last, ("z", "y"), up)
     after = lax.ppermute(kvb_first, ("z", "y"), down)
-    gated_b = call(
-        functools.partial(window_kernel, count=blocks),
-        shaped(rows, LANES),
-        [],
-        {0, 5},
-        {1, 2, 3, 4, 6},
-        place, qb, kvb, before, after, sink_b, gb,
-        name="windowed", flops=4 * 2 * rows * 576 * 64,
-    )
-    n_q = n_y * rows
-    n_k = n_z * rows
+    n_q = n_z * rows
+    n_k = n_y * rows
     tile = 512
     chunk = 256
     steps = 2 * n_q // tile
     parts = call(
         functools.partial(attend_kernel, tile=tile, chunk=chunk),
-        shaped(n_y, rows + STAT_ROWS, LANES),
+        shaped(n_z, rows + STAT_ROWS, LANES),
         [
             pltpu.VMEM((n_k, LANES), BF16),
             pltpu.VMEM((n_k // chunk, HEAD, chunk), BF16),
@@ -399,10 +399,29 @@
         ],
         {},
         {0, 1},
-        q_all, kv_all.reshape(n_k, LANES),
+        q_all.reshape(n_q, LANES), kv_all,
         name="attend", flops=4 * 2 * n_q * n_k * 64,
     )
-    back = lax.all_to_all(parts, "y", 0, 0, tiled=True)
+    parts, normed = lax.optimization_barrier((parts, normed))
+    back = lax.all_to_all(parts, "z", 0, 0, tiled=True)
+    ga, gb = call(
+        gate_kernel,
+        (shaped(rows, LANES, dtype=F32), shaped(rows, LANES, dtype=F32)),
+        [],
+        {},
+        {0, 1, 2},
+        normed, w_ga, w_gb,
+        name="gates", flops=2 * rows * width * tp * 256,
+    )
+    gated_b = call(
+        functools.partial(window_kernel, count=blocks),
+        shaped(rows, LANES),
+        [],
+        {0, 5},
+        {1, 2, 3, 4, 6},
+        place, qb, kvb, before, after, sink_b, gb,
+        name="windowed", flops=4 * 2 * rows * 576 * 64,
+    )
     piece = shaped(n_x, rows // tp, out_a.shape[1])
     kept, sent = call(
         combine_kernel,

time: 135 us -> 139 us (1.030); the launches traced: 137 us -> 139 us
  local copies, waits for them, and re-layouts: 0.01 us -> 2.09 us
  blocking collectives: 66.9 us -> 68.6 us
  starting transfers between devices: 36.1 us -> 34.5 us
    all_to_all x2, waiting for transfers between devices: 0.01 us -> 6.59 us  [the longest x1 6.59 us: body(): back = lax.all_to_all(parts, 'z', 0, 0, tiled=True)]
    ppermute x1, waiting for transfers between devices: 4.87 us -> 1.67 us  [body(): after = lax.ppermute(kvb_first, ('z', 'y'), down)]
    ppermute x1, waiting for transfers between devices: 3.11 us -> 0.01 us  [body(): before = lax.ppermute(kvb_last, ('z', 'y'), up)]
    unnamed x4 -> x8, local copies, waits for them, and re-layouts: 0.01 us -> 2.09 us
    ppermute x1, starting transfers between devices: 10.2 us -> 8.41 us  [body(): got = lax.ppermute(sent, 'core', [(0, 1), (1, 0)])]
    all_to_all x1, blocking collectives: 33.3 us -> 35 us  [body(): arrived = lax.all_to_all(paired, 'x', 0, 0, tiled=True)]
    pallas_call x4 -> x5, Pallas kernels: 21.7 us -> 21.1 us  [call(): pl.pallas_call(kernel, out_shape=outs, in_specs=specs, out_specs=tuple((p...]
  transfers between devices with their start and end apart: 6 -> 6, of which waited for: 4 -> 4; matrix products, arithmetic and copies ran while one was open for 0% -> 0% of each run, Pallas kernels for 1% -> 2%
where the time goes in v1:
time: 139 us
  blocking collectives  68.6 us (49%)
  starting transfers between devices  34.5 us (25%)
  Pallas kernels  21.1 us (15%)
  waiting for transfers between devices  11 us (8%)
  local copies, waits for them, and re-layouts  2.09 us (2%)
  other arithmetic  1.6 us (1%)
    all_to_all x1, blocking collectives, body(): arrived = lax.all_to_all(paired, 'x', 0, 0, tiled=True)  35 us
    all_gather x1, blocking collectives, body(): kv_all = lax.all_gather(kv, 'y', axis=0, tiled=True)  22.1 us
    pallas_call x5, Pallas kernels, call(): pl.pallas_call(kernel, out_shape=outs, in_specs=specs, out_specs=tuple((p...  21.1 us
    all_gather x1, blocking collectives, body(): mine = lax.all_gather(tokens, 'x', axis=0)  11.5 us
    ppermute x1, starting transfers between devices, body(): other = lax.ppermute(mine, 'core', [(0, 1), (1, 0)])  10.5 us
    ppermute x1, starting transfers between devices, body(): got = lax.ppermute(sent, 'core', [(0, 1), (1, 0)])  8.41 us
    all_to_all x1, starting transfers between devices, body(): back = lax.all_to_all(parts, 'z', 0, 0, tiled=True)  6.74 us
    all_to_all x1, waiting for transfers between devices, body(): back = lax.all_to_all(parts, 'z', 0, 0, tiled=True)  6.59 us
  transfers between devices with their start and end apart: 6, of which 4 were waited for; matrix products, arithmetic and copies ran while one was open for 0% of the time, Pallas kernels for 2%

profile of v1, /device:TPU:1, one launch (start us, length us, event | category | flops | bytes accessed | tf_op | source)
XLA Modules:
  0.0 139.1 jit_solution(11236415193883925015)
XLA Ops:
  0.0 11.5 %all-gather = bf16[1280,256]{1,0:T(8,128)(2,1)S(1)} all-gather(bf16[320,256]{1,0:T(8,128)(2,1)} %param.17), channel_id=2, replica_groups=mesh['z'=8,'y'=8,'x'=4,'core'=2] {'x'}, dimensions={0}, use_global_device_ids=true | all-gather | bytes 819200 | tf_op jit(solution)/shard_map/all_gather | solution.py:352
  11.5 10.5 %collective-permute-start = (bf16[4,320,256]{2,1,0:T(8,128)(2,1)S(1)}, bf16[4,320,256]{2,1,0:T(8,128)(2,1)S(1)}, u32[]{:S(2)}, u32[]{:S(2)}) collective-permute-start(bf16[4,320,256]{2,1,0:T(8,128)(2,1)S(1)} %bitcast.9), channel_id=1, source_target_pairs={{0,1},{1,0},{2,3},{3,2},{4,5},{5,4},{6,7},{7,6},{8,9},{9,8},{10,11... | collective-permute-start | bytes 1966088 | tf_op jit(solution)/shard_map/ppermute | solution.py:353
  22.0 0.6 pad_add_fusion.place_ref
  22.6 1.1 collective-permute-done.other_ref
  23.7 4.6 %project.1 = (bf16[8,320,128]{2,1,0:T(8,128)(2,1)}, bf16[320,128]{1,0:T(8,128)(2,1)S(1)}, bf16[320,128]{1,0:T(8,128)(2,1)S(1)}, bf16[320,128]{1,0:T(8,128)(2,1)S...) custom-call(s32[2]{0:T(128)} %pad_add_fusion.place_ref, ...), custom_call_target="tpu_custom_call" | custom-call | flops 671088640 | bytes 1048576 | tf_op jit(solution)/shard_map/project/pallas_call | solution.py:319
  28.3 5.0 %all-to-all-start = ((bf16[8,320,128]{2,1,0:T(8,128)(2,1)}), bf16[8,320,128]{2,1,0:T(8,128)(2,1)S(1)}, u32[]{:S(2)}, u32[]{:S(2)}) async-start(bf16[8,320,128]{2,1,0:T(8,128)(2,1)} %get-tuple-element.18), calls=%async_computation | async-start | bytes 1310720 | tf_op jit(solution)/shard_map/all_to_all | solution.py:376
  33.4 22.1 %all_gather.11.kv_ref = bf16[2560,128]{1,0:T(8,128)(2,1)S(1)} all-gather(bf16[320,128]{1,0:T(8,128)(2,1)S(1)} %get-tuple-element.19), channel_id=1, replica_groups=mesh['z'=8,'y'=8,'x'=4,'core'=2] {'y'}, dimensions={0}, use_global_device_ids=true | all-gather | bytes 737280 | tf_op jit(solution)/shard_map/all_gather | solution.py:377
  55.4 12.0 %attend.1 = bf16[8,344,128]{2,1,0:T(8,128)(2,1)} custom-call(bf16[2560,128]{1,0:T(8,128)(2,1)S(1)} %bitcast.11, bf16[2560,128]{1,0:T(8,128)(2,1)S(1)} %all_gather.11.kv_ref), custom_call_target="tpu_custom_call" | custom-call | flops 3355443200 | bytes 1048576 | tf_op jit(solution)/shard_map/attend/pallas_call | solution.py:319
  67.4 6.7 %all-to-all-start.1 = ((bf16[8,344,128]{2,1,0:T(8,128)(2,1)}), bf16[8,344,128]{2,1,0:T(8,128)(2,1)S(1)}, u32[]{:S(2)}, u32[]{:S(2)}) async-start(bf16[8,344,128]{2,1,0:T(8,128)(2,1)} %attend.1), calls=%async_computation.1 | async-start | bytes 1409024 | tf_op jit(solution)/shard_map/all_to_all | solution.py:406
  74.2 2.4 %collective-permute-start.1 = (bf16[128,128]{1,0:T(8,128)(2,1)S(1)}, bf16[128,128]{1,0:T(8,128)(2,1)S(1)}, u32[]{:S(2)}, u32[]{:S(2)}) collective-permute-start(bf16[128,128]{1,0:T(8,128)(2,1)S(1)} %get-tuple-element.26), channel_id=1, source_target_pairs={{0,8},{8,16},{16,24},{24,32},{32,40},{40,48},{48,56},{56,64},{64,7... | collective-permute-start | bytes 98312 | tf_op jit(solution)/shard_map/ppermute | solution.py:380
  76.6 0.0 copy-start
  76.6 1.4 %collective-permute-start.2 = (bf16[128,128]{1,0:T(8,128)(2,1)S(1)}, bf16[128,128]{1,0:T(8,128)(2,1)S(1)}, u32[]{:S(2)}, u32[]{:S(2)}) collective-permute-start(bf16[128,128]{1,0:T(8,128)(2,1)S(1)} %get-tuple-element.27), channel_id=1, source_target_pairs={{8,0},{16,8},{24,16},{32,24},{40,32},{48,40},{56,48},{64,56},{72,6... | collective-permute-start | bytes 98312 | tf_op jit(solution)/shard_map/ppermute | solution.py:381
  78.1 1.0 copy-done.2
  79.1 1.0 copy-done.3
  80.1 0.5 gates.1
  80.7 1.7 %collective-permute-done.2.next_ref = bf16[128,128]{1,0:T(8,128)(2,1)S(1)} collective-permute-done((bf16[128,128]{1,0:T(8,128)(2,1)S(1)}, bf16[128,128]{1,0:T(8,128)(2,1)S(1)}, u32[]{:S(2)}, u32[]{:S(2)}) %collective-permute-start.2) | collective-permute-done | bytes 32800 | tf_op jit(solution)/shard_map/ppermute | solution.py:381
  82.4 1.8 %windowed.1.gated_b_ref = bf16[320,128]{1,0:T(8,128)(2,1)S(1)} custom-call(s32[2]{0:T(128)} %pad_add_fusion.place_ref, bf16[320,128]{1,0:T(8,128)(2,1)S(1)} %get-tuple-element.24.q_ref, bf16[320,128]{1,0:T(8,128)(2,1)S(1)} %get-tuple-element.25.mid_ref, bf16[128,128]{1,0:T(8,128)(2,1)S(1)} %collective-permute-done.1.prev_ref, ...), custom_call_target="tpu_custom_call" | custom-call | flops 94371840 | bytes 1048576 | tf_op jit(solution)/shard_map/windowed/pallas_call | solution.py:319
  84.1 6.6 %all-to-all-done.1.part_ref = bf16[8,344,128]{2,1,0:T(8,128)(2,1)S(1)} async-done(((bf16[8,344,128]{2,1,0:T(8,128)(2,1)}), bf16[8,344,128]{2,1,0:T(8,128)(2,1)S(1)}, u32[]{:S(2)}, u32[]{:S(2)}) %all-to-all-start.1) | async-done | bytes 704544 | tf_op jit(solution)/shard_map/all_to_all | solution.py:406
  90.7 2.2 %combine.1 = (bf16[4,40,2048]{2,1,0:T(8,128)(2,1)S(1)}, bf16[4,40,2048]{2,1,0:T(8,128)(2,1)S(1)}) custom-call(s32[2]{0:T(128)} %pad_add_fusion.place_ref, bf16[8,344,128]{2,1,0:T(8,128)(2,1)S(1)} %all-to-all-done.1.part_ref, f32[320,128]{1,0:T(8,128)S(1)} %get-tuple-element.23.ga_ref, bf16[320,128]{1,0:T(8,128)(2,1)S(1)} %windowed.1.gated_b_ref, ...), custom_call_target="tpu_custom_call" | custom-call | flops 335544320 | bytes 1048576 | tf_op jit(solution)/shard_map/combine/pallas_call | solution.py:319
  92.9 8.4 %collective-permute-start.3 = (bf16[4,40,2048]{2,1,0:T(8,128)(2,1)S(1)}, bf16[4,40,2048]{2,1,0:T(8,128)(2,1)S(1)}, u32[]{:S(2)}, u32[]{:S(2)}) collective-permute-start(bf16[4,40,2048]{2,1,0:T(8,128)(2,1)S(1)} %get-tuple-element.30), channel_id=1, source_target_pairs={{0,1},{1,0},{2,3},{3,2},{4,5},{5,4},{6,7},{7,6},{8,9},{9,8},{10,11... | collective-permute-start | bytes 1966088 | tf_op jit(solution)/shard_map/ppermute | solution.py:435
  101.4 1.7 %collective-permute-done.3 = bf16[4,40,2048]{2,1,0:T(8,128)(2,1)S(1)} collective-permute-done((bf16[4,40,2048]{2,1,0:T(8,128)(2,1)S(1)}, bf16[4,40,2048]{2,1,0:T(8,128)(2,1)S(1)}, u32[]{:S(2)}, u32[]{:S(2)}) %collective-permute-start.3) | collective-permute-done | bytes 655392 | tf_op jit(solution)/shard_map/ppermute | solution.py:435
  103.1 0.2 add_convert_fusion
  103.3 35.0 %all_to_all.15 = bf16[4,40,2048]{2,1,0:T(8,128)(2,1)S(1)} all-to-all(bf16[4,40,2048]{2,1,0:T(8,128)(2,1)S(1)} %add_convert_fusion), channel_id=1, replica_groups=mesh['z'=8,'y'=8,'x'=4,'core'=2] {'x'}, dimensions={0} | all-to-all | bytes 1310720 | tf_op jit(solution)/shard_map/all_to_all | solution.py:437
  138.3 0.8 reduce_sum.12
  (7 shorter events, 0.0 us)
Async XLA Ops:
  11.5 12.2 %collective-permute-start = (bf16[4,320,256]{2,1,0:T(8,128)(2,1)S(1)}, bf16[4,320,256]{2,1,0:T(8,128)(2,1)S(1)}, u32[]{:S(2)}, u32[]{:S(2)}) collective-permute-start(bf16[4,320,256]{2,1,0:T(8,128)(2,1)S(1)} %bitcast.9), channel_id=1, source_target_pairs={{0,1},{1,0},{2,3},{3,2},{4,5},{5,4},{6,7},{7,6},{8,9},{9,8},{10,11... | collective-permute-start | bytes 1966088 | tf_op jit(solution)/shard_map/ppermute | solution.py:353
  28.3 27.1 %all-to-all-start = ((bf16[8,320,128]{2,1,0:T(8,128)(2,1)}), bf16[8,320,128]{2,1,0:T(8,128)(2,1)S(1)}, u32[]{:S(2)}, u32[]{:S(2)}) async-start(bf16[8,320,128]{2,1,0:T(8,128)(2,1)} %get-tuple-element.18), calls=%async_computation | async-start | bytes 1310720 | tf_op jit(solution)/shard_map/all_to_all | solution.py:376
  67.4 23.3 %all-to-all-start.1 = ((bf16[8,344,128]{2,1,0:T(8,128)(2,1)}), bf16[8,344,128]{2,1,0:T(8,128)(2,1)S(1)}, u32[]{:S(2)}, u32[]{:S(2)}) async-start(bf16[8,344,128]{2,1,0:T(8,128)(2,1)} %attend.1), calls=%async_computation.1 | async-start | bytes 1409024 | tf_op jit(solution)/shard_map/all_to_all | solution.py:406
  74.2 6.5 %collective-permute-start.1 = (bf16[128,128]{1,0:T(8,128)(2,1)S(1)}, bf16[128,128]{1,0:T(8,128)(2,1)S(1)}, u32[]{:S(2)}, u32[]{:S(2)}) collective-permute-start(bf16[128,128]{1,0:T(8,128)(2,1)S(1)} %get-tuple-element.26), channel_id=1, source_target_pairs={{0,8},{8,16},{16,24},{24,32},{32,40},{40,48},{48,56},{56,64},{64,7... | collective-permute-start | bytes 98312 | tf_op jit(solution)/shard_map/ppermute | solution.py:380
  76.6 14.1 %copy-start = (bf16[128,2048]{1,0:T(8,128)(2,1)S(1)}, bf16[128,2048]{1,0:T(8,128)(2,1)}, u32[]{:S(2)}) copy-start(bf16[128,2048]{1,0:T(8,128)(2,1)} %wa_ref.3) | copy-start | bytes 1572868
  76.6 14.1 %copy-start.1 = (bf16[128,2048]{1,0:T(8,128)(2,1)S(1)}, bf16[128,2048]{1,0:T(8,128)(2,1)}, u32[]{:S(2)}) copy-start(bf16[128,2048]{1,0:T(8,128)(2,1)} %wb_ref.3) | copy-start | bytes 1572868
  76.6 5.7 %collective-permute-start.2 = (bf16[128,128]{1,0:T(8,128)(2,1)S(1)}, bf16[128,128]{1,0:T(8,128)(2,1)S(1)}, u32[]{:S(2)}, u32[]{:S(2)}) collective-permute-start(bf16[128,128]{1,0:T(8,128)(2,1)S(1)} %get-tuple-element.27), channel_id=1, source_target_pairs={{8,0},{16,8},{24,16},{32,24},{40,32},{48,40},{56,48},{64,56},{72,6... | collective-permute-start | bytes 98312 | tf_op jit(solution)/shard_map/ppermute | solution.py:381
  78.1 1.0 copy-start.2
  79.1 1.0 copy-start.3
  92.9 10.1 %collective-permute-start.3 = (bf16[4,40,2048]{2,1,0:T(8,128)(2,1)S(1)}, bf16[4,40,2048]{2,1,0:T(8,128)(2,1)S(1)}, u32[]{:S(2)}, u32[]{:S(2)}) collective-permute-start(bf16[4,40,2048]{2,1,0:T(8,128)(2,1)S(1)} %get-tuple-element.30), channel_id=1, source_target_pairs={{0,1},{1,0},{2,3},{3,2},{4,5},{5,4},{6,7},{7,6},{8,9},{9,8},{10,11... | collective-permute-start | bytes 1966088 | tf_op jit(solution)/shard_map/ppermute | solution.py:435

commit v2 on v1

--- a/solution.py
+++ b/solution.py
@@ -7,6 +7,7 @@
 from jax.experimental import pallas as pl
 from jax.experimental.pallas import tpu as pltpu
 from jax.sharding import Mesh, PartitionSpec as P
+
 
 GRID = 64
 WINDOW = 128
@@ -17,6 +18,8 @@
 BOUND = 69.0
 SHIFT = 55.0
 STAT_ROWS = 24
+SP = ("z", "yh", "yl")
+TP = ("x", "core")
 F32 = jnp.float32
 BF16 = jnp.bfloat16
 
@@ -55,22 +58,25 @@
     return v / (1.0 + jnp.exp(-v))
 
 
-def project_kernel(
-    place_ref, mine_ref, other_ref, gain_ref, qgain_ref, kgain_ref, col_ref, row_ref,
-    wqa, wka, wva, wqb, wkb, wvb,
-    q_out, kv_out, qb_out, kvb_out, first_out, last_out, h_out,
-    h_s, wide_s, narrow_s, row_s, sems,
+def rotated(n, row_s, col_ref):
+    rows = n.shape[0]
+    grid_rows = rows // GRID
+    cos = jnp.concatenate([row_s[r : r + 1] + col_ref[0] for r in range(grid_rows)], axis=0)
+    sin = jnp.concatenate([row_s[8 + r : 9 + r] + col_ref[1] for r in range(grid_rows)], axis=0)
+    first = (lax.broadcasted_iota(jnp.int32, (rows, LANES), 1) % 32) < 16
+    partner = jnp.where(first, -pltpu.roll(n, LANES - 16, 1), pltpu.roll(n, 16, 1))
+    return n * cos + partner * sin
+
+
+def key_kernel(
+    place_ref, mine_ref, other_ref, gain_ref, kgain_ref, col_ref, row_ref, wka, wva,
+    kv_out, h_out, h_s, narrow_s, row_s, sems,
 ):
     core = place_ref[0]
-    wide = [wqa, wqb]
-    narrow = [wka, wva, wkb, wvb]
-    copies = [pltpu.make_async_copy(row_ref.at[place_ref[1]], row_s, sems.at[6])]
+    copies = [pltpu.make_async_copy(row_ref.at[place_ref[1]], row_s, sems.at[2])]
     copies += [
         pltpu.make_async_copy(ref, narrow_s.at[i * HEAD : (i + 1) * HEAD], sems.at[i])
-        for i, ref in enumerate(narrow)
-    ]
-    copies += [
-        pltpu.make_async_copy(ref, wide_s.at[i], sems.at[4 + i]) for i, ref in enumerate(wide)
+        for i, ref in enumerate((wka, wva))
     ]
     for copy in copies:
         copy.start()
@@ -94,24 +100,35 @@
     h_out[...] = normed
     for copy in copies:
         copy.wait()
-    both_kv = dot_t(normed, narrow_s[...])
+    kv = dot_t(normed, narrow_s[...]).astype(BF16).astype(F32)
+    low = lax.broadcasted_iota(jnp.int32, (rows, LANES), 1) < HEAD
+    k_only = jnp.where(low, kv, 0.0)
+    sq = jnp.sum(k_only * k_only, axis=1, keepdims=True)
+    kgain = jnp.concatenate([kgain_ref[...], kgain_ref[...]], axis=1)
+    ka = rotated(k_only * lax.rsqrt(sq / HEAD + EPSILON) * kgain, row_s, col_ref)
+    kv_out[...] = jnp.where(low, ka, kv).astype(BF16)
+
+
+def query_kernel(
+    place_ref, h_ref, qgain_ref, col_ref, row_ref, wqa, wqb, wkb, wvb,
+    q_out, qb_out, kvb_out, first_out, last_out, wide_s, narrow_s, row_s, sems,
+):
+    copies = [pltpu.make_async_copy(row_ref.at[place_ref[1]], row_s, sems.at[4])]
+    copies += [
+        pltpu.make_async_copy(ref, wide_s.at[i], sems.at[i]) for i, ref in enumerate((wqa, wqb))
+    ]
+    copies += [
+        pltpu.make_async_copy(ref, narrow_s.at[i * HEAD : (i + 1) * HEAD], sems.at[2 + i])
+        for i, ref in enumerate((wkb, wvb))
+    ]
+    for copy in copies:
+        copy.start()
+    for copy in copies:
+        copy.wait()
+    normed = h_ref[...]
+    rows = normed.shape[0]
     both_q = dot(normed, jnp.concatenate([wide_s[0], wide_s[1]], axis=1))
-    qb_out[...] = both_q[:, LANES:].astype(BF16)
-    kvb = both_kv[:, LANES:].astype(BF16)
-    kvb_out[...] = kvb
-    first_out[...] = kvb[:WINDOW]
-    last_out[...] = kvb[rows - WINDOW :]
-    grid_rows = rows // GRID
-    cos = jnp.concatenate([row_s[r : r + 1] + col_ref[0] for r in range(grid_rows)], axis=0)
-    sin = jnp.concatenate([row_s[8 + r : 9 + r] + col_ref[1] for r in range(grid_rows)], axis=0)
-    lane = lax.broadcasted_iota(jnp.int32, (rows, LANES), 1)
-    first = (lane % 32) < 16
-    low = lane < HEAD
-
-    def turned(n):
-        partner = jnp.where(first, -pltpu.roll(n, LANES - 16, 1), pltpu.roll(n, 16, 1))
-        return n * cos + partner * sin
-
+    low = lax.broadcasted_iota(jnp.int32, (rows, LANES), 1) < HEAD
     v = both_q[:, :LANES].astype(BF16).astype(F32)
     square = v * v
     sum_low = jnp.sum(jnp.where(low, square, 0.0), axis=1, keepdims=True)
@@ -119,15 +136,14 @@
     rs_low = lax.rsqrt(sum_low / HEAD + EPSILON)
     rs_high = lax.rsqrt(sum_high / HEAD + EPSILON)
     qgain = jnp.concatenate([qgain_ref[0:1, :], qgain_ref[1:2, :]], axis=1)
-    qa = turned(v * jnp.where(low, rs_low, rs_high) * qgain).astype(BF16)
+    qa = rotated(v * jnp.where(low, rs_low, rs_high) * qgain, row_s, col_ref).astype(BF16)
     for i in range(q_out.shape[0]):
         q_out[i] = qa
-    kv = both_kv[:, :LANES].astype(BF16).astype(F32)
-    k_only = jnp.where(low, kv, 0.0)
-    sq = jnp.sum(k_only * k_only, axis=1, keepdims=True)
-    kgain = jnp.concatenate([kgain_ref[...], kgain_ref[...]], axis=1)
-    ka = turned(k_only * lax.rsqrt(sq / HEAD + EPSILON) * kgain)
-    kv_out[...] = jnp.where(low, ka, kv).astype(BF16)
+    qb_out[...] = both_q[:, LANES:].astype(BF16)
+    kvb = dot_t(normed, narrow_s[...]).astype(BF16)
+    kvb_out[...] = kvb
+    first_out[...] = kvb[:WINDOW]
+    last_out[...] = kvb[rows - WINDOW :]
 
 
 def gate_kernel(h_ref, wa_ref, wb_ref, ga_out, gb_out):
@@ -305,7 +321,7 @@
         sent_ref[i] = out_s[2 * i + 1 - core]
 
 
-def call(kernel, outs, scratch, smem, near, *args, name, flops=0, far=()):
+def call(kernel, outs, scratch, smem, near, *args, flops=0, far=()):
     args = [
         pltpu.with_memory_space_constraint(a, pltpu.VMEM) if i in near else a
         for i, a in enumerate(args)
@@ -328,7 +344,6 @@
         scratch_shapes=scratch,
         compiler_params=pltpu.CompilerParams(vmem_limit_bytes=56 * 2**20),
         cost_estimate=pl.CostEstimate(flops=flops, bytes_accessed=2**20, transcendentals=0),
-        name=name,
     )(*args)
 
 
@@ -341,44 +356,59 @@
     out_a, out_b,
 ):
     rows, width = tokens.shape
-    n_z, n_y, n_x = (lax.axis_size(a) for a in ("z", "y", "x"))
+    n_z, n_x = (lax.axis_size(a) for a in ("z", "x"))
+    n_y = lax.axis_size("yh") * lax.axis_size("yl")
     blocks = n_z * n_y
     tp = 2 * n_x
-    s_index = lax.axis_index("z") * n_y + lax.axis_index("y")
+    s_index = lax.axis_index(SP)
     core = lax.axis_index("core")
     place = jnp.stack([core, s_index]).astype(jnp.int32)
     row_table, col_table = rotary_tables(blocks * rows, blocks)
 
     mine = lax.all_gather(tokens, "x", axis=0)
     other = lax.ppermute(mine, "core", [(0, 1), (1, 0)])
-    q8, kv, qb, kvb, kvb_first, kvb_last, normed = call(
-        project_kernel,
-        (
-            shaped(n_z, rows, LANES), shaped(rows, LANES),
-            shaped(rows, LANES), shaped(rows, LANES),
-            shaped(WINDOW, LANES), shaped(WINDOW, LANES),
-            shaped(rows, tp * width),
-        ),
+    col_table = jnp.asarray(col_table)
+    row_table = jnp.asarray(row_table)
+    kv, normed = call(
+        key_kernel,
+        (shaped(rows, LANES), shaped(rows, tp * width)),
         [
             pltpu.VMEM((tp, rows, width), BF16),
-            pltpu.VMEM((2, tp * width, LANES), BF16),
-            pltpu.VMEM((4 * HEAD, tp * width), BF16),
+            pltpu.VMEM((2 * HEAD, tp * width), BF16),
             pltpu.VMEM((16, LANES), F32),
-            pltpu.SemaphoreType.DMA((7,)),
+            pltpu.SemaphoreType.DMA((3,)),
         ],
         {0},
         {1, 2},
-        place, mine, other, norm_gain.reshape(tp, 1, width), qgain_a, kgain_a,
-        jnp.asarray(col_table), jnp.asarray(row_table),
-        w_qa, w_ka.T, w_va.T, w_qb, w_kb.T, w_vb.T,
-        name="project", flops=2 * rows * width * tp * 512, far=set(range(7, 14)),
+        place, mine, other, norm_gain.reshape(tp, 1, width), kgain_a, col_table, row_table,
+        w_ka.T, w_va.T,
+        flops=2 * rows * width * tp * 128, far={6, 7, 8},
+    )
+    kv_far = lax.ppermute(kv, "yh", [(0, 1), (1, 0)])
+    q8, qb, kvb, kvb_first, kvb_last = call(
+        query_kernel,
+        (
+            shaped(n_z, rows, LANES), shaped(rows, LANES), shaped(rows, LANES),
+            shaped(WINDOW, LANES), shaped(WINDOW, LANES),
+        ),
+        [
+            pltpu.VMEM((2, tp * width, LANES), BF16),
+            pltpu.VMEM((2 * HEAD, tp * width), BF16),
+            pltpu.VMEM((16, LANES), F32),
+            pltpu.SemaphoreType.DMA((5,)),
+        ],
+        {0},
+        {1},
+        place, normed, qgain_a, col_table, row_table, w_qa, w_qb, w_kb.T, w_vb.T,
+        flops=2 * rows * width * tp * 384, far={4, 5, 6, 7, 8},
     )
     q_all = lax.all_to_all(q8, "z", 0, 0, tiled=True)
-    kv_all = lax.all_gather(kv, "y", axis=0, tiled=True)
+    kv_pair = jnp.concatenate([kv, kv_far], axis=0)
+    kv_all = lax.all_gather(kv_pair, "yl", axis=0, tiled=True)
     up = [(i, i + 1) for i in range(blocks - 1)]
     down = [(i + 1, i) for i in range(blocks - 1)]
-    before = lax.ppermute(kvb_last, ("z", "y"), up)
-    after = lax.ppermute(kvb_first, ("z", "y"), down)
+    before = lax.ppermute(kvb_last, SP, up)
+    after = lax.ppermute(kvb_first, SP, down)
     n_q = n_z * rows
     n_k = n_y * rows
     tile = 512
@@ -400,7 +430,7 @@
         {},
         {0, 1},
         q_all.reshape(n_q, LANES), kv_all,
-        name="attend", flops=4 * 2 * n_q * n_k * 64,
+        flops=4 * 2 * n_q * n_k * 64,
     )
     parts, normed = lax.optimization_barrier((parts, normed))
     back = lax.all_to_all(parts, "z", 0, 0, tiled=True)
@@ -411,7 +441,7 @@
         {},
         {0, 1, 2},
         normed, w_ga, w_gb,
-        name="gates", flops=2 * rows * width * tp * 256,
+        flops=2 * rows * width * tp * 256,
     )
     gated_b = call(
         functools.partial(window_kernel, count=blocks),
@@ -420,7 +450,7 @@
         {0, 5},
         {1, 2, 3, 4, 6},
         place, qb, kvb, before, after, sink_b, gb,
-        name="windowed", flops=4 * 2 * rows * 576 * 64,
+        flops=4 * 2 * rows * 576 * 64,
     )
     piece = shaped(n_x, rows // tp, out_a.shape[1])
     kept, sent = call(
@@ -430,7 +460,7 @@
         {0},
         {1, 2, 3, 4, 5},
         place, back, ga, gated_b, out_a, out_b,
-        name="combine", flops=2 * rows * 256 * 2048,
+        flops=2 * rows * 256 * 2048,
     )
     got = lax.ppermute(sent, "core", [(0, 1), (1, 0)])
     paired = (kept.astype(F32) + got.astype(F32)).astype(BF16)
@@ -439,13 +469,10 @@
 
 
 def solution(mesh):
-    n_sp, n_tp = (mesh.shape["sp"], mesh.shape["tp"])
-    n_z = 8
-    fine = Mesh(
-        np.asarray(mesh.devices).reshape(n_z, n_sp // n_z, n_tp // 2, 2), ("z", "y", "x", "core")
-    )
-    sp = ("z", "y")
-    tp = ("x", "core")
+    n_tp = mesh.shape["tp"]
+    fine = Mesh(np.asarray(mesh.devices).reshape(8, 2, 4, n_tp // 2, 2), (*SP, *TP))
+    sp = SP
+    tp = TP
     placed = (
         P(sp, tp), P(), P(None, tp), P(None, tp), P(None, tp), P(tp, None), P(tp, None),
         P(None, tp), P(None, tp), P(None, tp), P(tp), P(None, tp), P(None, tp), P(tp, None),

time: 139 us -> 144 us (1.036)
  blocking collectives: 68.6 us -> 61.2 us
  waiting for transfers between devices: 11 us -> 16.4 us
  starting transfers between devices: 34.5 us -> 38.1 us
  Pallas kernels: 21.1 us -> 23.3 us
    ppermute x2 -> x3, starting transfers between devices: 3.86 us -> 10.4 us  [the longest x1 7.44 us: body(): kv_far = lax.ppermute(kv, 'yh', [(0, 1), (1, 0)])]
    all_gather x1, blocking collectives: 22.1 us -> 16.4 us  [body(): kv_all = lax.all_gather(kv_pair, 'yl', axis=0, tiled=True)]
    all_to_all x1, waiting for transfers between devices: 6.59 us -> 11 us  [body(): back = lax.all_to_all(parts, 'z', 0, 0, tiled=True)]
    ppermute x1, starting transfers between devices: 8.41 us -> 5.85 us  [body(): got = lax.ppermute(sent, 'core', [(0, 1), (1, 0)])]
    pallas_call x5 -> x6, Pallas kernels: 21.1 us -> 23.3 us  [call(): pl.pallas_call(kernel, out_shape=outs, in_specs=specs, out_specs=tuple((p...]
    all_to_all x1, blocking collectives: 35 us -> 33.3 us  [body(): arrived = lax.all_to_all(paired, 'x', 0, 0, tiled=True)]
  transfers between devices with their start and end apart: 6 -> 7, of which waited for: 4 -> 5; matrix products, arithmetic and copies ran while one was open for 0% -> 0% of each run, Pallas kernels for 2% -> 2%
where the time goes in v2:
time: 144 us; the launch traced here: 143 us
  blocking collectives  61.2 us (42%)
  starting transfers between devices  38.1 us (26%)
  Pallas kernels  23.3 us (16%)
  waiting for transfers between devices  16.4 us (11%)
  local copies, waits for them, and re-layouts  2.09 us (1%)
  other arithmetic  1.64 us (1%)
    all_to_all x1, blocking collectives, body(): arrived = lax.all_to_all(paired, 'x', 0, 0, tiled=True)  33.3 us
    pallas_call x6, Pallas kernels, call(): pl.pallas_call(kernel, out_shape=outs, in_specs=specs, out_specs=tuple((p...  23.3 us
    all_gather x1, blocking collectives, body(): kv_all = lax.all_gather(kv_pair, 'yl', axis=0, tiled=True)  16.4 us
    all_gather x1, blocking collectives, body(): mine = lax.all_gather(tokens, 'x', axis=0)  11.5 us
    all_to_all x1, waiting for transfers between devices, body(): back = lax.all_to_all(parts, 'z', 0, 0, tiled=True)  11 us
    ppermute x1, starting transfers between devices, body(): other = lax.ppermute(mine, 'core', [(0, 1), (1, 0)])  10.5 us
    ppermute x1, starting transfers between devices, body(): kv_far = lax.ppermute(kv, 'yh', [(0, 1), (1, 0)])  7.44 us
    all_to_all x1, starting transfers between devices, body(): back = lax.all_to_all(parts, 'z', 0, 0, tiled=True)  6.36 us
  transfers between devices with their start and end apart: 7, of which 5 were waited for; matrix products, arithmetic and copies ran while one was open for 0% of the time, Pallas kernels for 2%

profile of v2, /device:TPU:1, one launch (start us, length us, event | category | flops | bytes accessed | tf_op | source)
XLA Modules:
  0.0 142.8 jit_solution(9097244329191295667)
XLA Ops:
  0.0 11.5 %all-gather = bf16[1280,256]{1,0:T(8,128)(2,1)S(1)} all-gather(bf16[320,256]{1,0:T(8,128)(2,1)} %param.17), channel_id=2, replica_groups=mesh['z'=8,'yh'=2,'yl'=4,'x'=4,'core'=2] {'x'}, dimensions={0}, use_global_device_ids=true | all-gather | bytes 819200 | tf_op jit(solution)/shard_map/all_gather | solution.py:368
  11.5 10.5 %collective-permute-start = (bf16[4,320,256]{2,1,0:T(8,128)(2,1)S(1)}, bf16[4,320,256]{2,1,0:T(8,128)(2,1)S(1)}, u32[]{:S(2)}, u32[]{:S(2)}) collective-permute-start(bf16[4,320,256]{2,1,0:T(8,128)(2,1)S(1)} %bitcast.9), channel_id=1, source_target_pairs={{0,1},{1,0},{2,3},{3,2},{4,5},{5,4},{6,7},{7,6},{8,9},{9,8},{10,11... | collective-permute-start | bytes 1966088 | tf_op jit(solution)/shard_map/ppermute | solution.py:369
  22.0 0.6 pad_add_fusion.place_ref
  22.6 1.0 collective-permute-done.other_ref
  23.7 2.6 %shard_map.163 = (bf16[320,128]{1,0:T(8,128)(2,1)S(1)}, bf16[320,2048]{1,0:T(8,128)(2,1)S(1)}) custom-call(s32[2]{0:T(128)} %pad_add_fusion.place_ref, bf16[4,320,256]{2,1,0:T(8,128)(2,1)S(1)} %bitcast.10, bf16[4,320,256]{2,1,0:T(8,128)(2,1)S(1)} %collective-permute-done.other_ref, f32[8,1,256]{2,1,0:T(1,128)} %bitcast.16, f32[1,64]{1,0:T(1,128)} %kgain_ref.1, ...), custom_call_target="tpu_custom_call" | custom-call | flops 167772160 | bytes 1048576 | tf_op jit(solution)/shard_map/pallas_call | solution.py:335
  26.3 4.1 %shard_map.164 = (bf16[8,320,128]{2,1,0:T(8,128)(2,1)}, bf16[320,128]{1,0:T(8,128)(2,1)S(1)}, bf16[320,128]{1,0:T(8,128)(2,1)S(1)}, bf16[128,128]{1,0:T(8,128)(2,1)S(1)}, bf16[128,128]{1,0:T(8,128)(2,1)S(1)}) custom-call(s32[2]{0:T(128)} %pad_add_fusion.place_ref, bf16[320,2048]{1,0:T(8,128)(2,1)S(1)} %get-tuple-element.22.h_ref, f32[2,64]{1,0:T(2,128)} %qgain_ref.1, ...), custom_call_target="tpu_custom_call" | custom-call | flops 503316480 | bytes 1048576 | tf_op jit(solution)/shard_map/pallas_call | solution.py:335
  30.5 5.1 %all-to-all-start = ((bf16[8,320,128]{2,1,0:T(8,128)(2,1)}), bf16[8,320,128]{2,1,0:T(8,128)(2,1)S(1)}, u32[]{:S(2)}, u32[]{:S(2)}) async-start(bf16[8,320,128]{2,1,0:T(8,128)(2,1)} %get-tuple-element.19), calls=%async_computation | async-start | bytes 1310720 | tf_op jit(solution)/shard_map/all_to_all | solution.py:405
  35.5 7.4 %collective-permute-start.1 = (bf16[320,128]{1,0:T(8,128)(2,1)S(1)}, bf16[320,128]{1,0:T(8,128)(2,1)S(1)}, u32[]{:S(2)}, u32[]{:S(2)}) collective-permute-start(bf16[320,128]{1,0:T(8,128)(2,1)S(1)} %get-tuple-element.20), channel_id=1, source_target_pairs={{0,32},{32,0},{1,33},{33,1},{2,34},{34,2},{3,35},{35,3},{4,36},{36... | collective-permute-start | bytes 245768 | tf_op jit(solution)/shard_map/ppermute | solution.py:387
  43.0 1.9 %collective-permute-done.1 = bf16[320,128]{1,0:T(8,128)(2,1)S(1)} collective-permute-done((bf16[320,128]{1,0:T(8,128)(2,1)S(1)}, bf16[320,128]{1,0:T(8,128)(2,1)S(1)}, u32[]{:S(2)}, u32[]{:S(2)}) %collective-permute-start.1) | collective-permute-done | bytes 81952 | tf_op jit(solution)/shard_map/ppermute | solution.py:387
  44.9 16.4 %all_gather.11.kv_ref = bf16[2560,128]{1,0:T(8,128)(2,1)S(1)} all-gather(bf16[640,128]{1,0:T(8,128)(2,1)S(1)} %pad_maximum_fusion), channel_id=1, replica_groups=mesh['z'=8,'yh'=2,'yl'=4,'x'=4,'core'=2] {'yl'}, dimensions={0}, use_global_device_ids=true | all-gather | bytes 819200 | tf_op jit(solution)/shard_map/all_gather | solution.py:407
  61.3 12.0 %shard_map.165 = bf16[8,344,128]{2,1,0:T(8,128)(2,1)} custom-call(bf16[2560,128]{1,0:T(8,128)(2,1)S(1)} %bitcast.11, bf16[2560,128]{1,0:T(8,128)(2,1)S(1)} %all_gather.11.kv_ref), custom_call_target="tpu_custom_call" | custom-call | flops 3355443200 | bytes 1048576 | tf_op jit(solution)/shard_map/pallas_call | solution.py:335
  73.3 6.4 %all-to-all-start.1 = ((bf16[8,344,128]{2,1,0:T(8,128)(2,1)}), bf16[8,344,128]{2,1,0:T(8,128)(2,1)S(1)}, u32[]{:S(2)}, u32[]{:S(2)}) async-start(bf16[8,344,128]{2,1,0:T(8,128)(2,1)} %shard_map.165), calls=%async_computation.1 | async-start | bytes 1409024 | tf_op jit(solution)/shard_map/all_to_all | solution.py:436
  79.7 1.5 %collective-permute-start.2 = (bf16[128,128]{1,0:T(8,128)(2,1)S(1)}, bf16[128,128]{1,0:T(8,128)(2,1)S(1)}, u32[]{:S(2)}, u32[]{:S(2)}) collective-permute-start(bf16[128,128]{1,0:T(8,128)(2,1)S(1)} %get-tuple-element.26), channel_id=1, source_target_pairs={{0,8},{8,16},{16,24},{24,32},{32,40},{40,48},{48,56},{56,64},{64,7... | collective-permute-start | bytes 98312 | tf_op jit(solution)/shard_map/ppermute | solution.py:410
  81.2 1.4 collective-permute-start.3
  82.6 1.0 copy-done.2
  83.7 1.0 copy-done.3
  85.3 0.7 collective-permute-done.3.next_ref
  86.0 1.8 %shard_map.167.gated_b_ref = bf16[320,128]{1,0:T(8,128)(2,1)S(1)} custom-call(s32[2]{0:T(128)} %pad_add_fusion.place_ref, bf16[320,128]{1,0:T(8,128)(2,1)S(1)} %get-tuple-element.24.q_ref, bf16[320,128]{1,0:T(8,128)(2,1)S(1)} %get-tuple-element.25.mid_ref, bf16[128,128]{1,0:T(8,128)(2,1)S(1)} %collective-permute-done.2.prev_ref, ...), custom_call_target="tpu_custom_call" | custom-call | flops 94371840 | bytes 1048576 | tf_op jit(solution)/shard_map/pallas_call | solution.py:335
  87.8 11.0 %all-to-all-done.1.part_ref = bf16[8,344,128]{2,1,0:T(8,128)(2,1)S(1)} async-done(((bf16[8,344,128]{2,1,0:T(8,128)(2,1)}), bf16[8,344,128]{2,1,0:T(8,128)(2,1)S(1)}, u32[]{:S(2)}, u32[]{:S(2)}) %all-to-all-start.1) | async-done | bytes 704544 | tf_op jit(solution)/shard_map/all_to_all | solution.py:436
  98.8 2.2 %shard_map.168 = (bf16[4,40,2048]{2,1,0:T(8,128)(2,1)S(1)}, bf16[4,40,2048]{2,1,0:T(8,128)(2,1)S(1)}) custom-call(s32[2]{0:T(128)} %pad_add_fusion.place_ref, bf16[8,344,128]{2,1,0:T(8,128)(2,1)S(1)} %all-to-all-done.1.part_ref, f32[320,128]{1,0:T(8,128)S(1)} %get-tuple-element.23.ga_ref, bf16[320,128]{1,0:T(8,128)(2,1)S(1)} %shard_map.167.gated_b_ref, ...), custom_call_target="tpu_custom_call" | custom-call | flops 335544320 | bytes 1048576 | tf_op jit(solution)/shard_map/pallas_call | solution.py:335
  101.0 5.9 %collective-permute-start.4 = (bf16[4,40,2048]{2,1,0:T(8,128)(2,1)S(1)}, bf16[4,40,2048]{2,1,0:T(8,128)(2,1)S(1)}, u32[]{:S(2)}, u32[]{:S(2)}) collective-permute-start(bf16[4,40,2048]{2,1,0:T(8,128)(2,1)S(1)} %get-tuple-element.30), channel_id=1, source_target_pairs={{0,1},{1,0},{2,3},{3,2},{4,5},{5,4},{6,7},{7,6},{8,9},{9,8},{10,11... | collective-permute-start | bytes 1966088 | tf_op jit(solution)/shard_map/ppermute | solution.py:465
  106.9 1.7 %collective-permute-done.4 = bf16[4,40,2048]{2,1,0:T(8,128)(2,1)S(1)} collective-permute-done((bf16[4,40,2048]{2,1,0:T(8,128)(2,1)S(1)}, bf16[4,40,2048]{2,1,0:T(8,128)(2,1)S(1)}, u32[]{:S(2)}, u32[]{:S(2)}) %collective-permute-start.4) | collective-permute-done | bytes 655392 | tf_op jit(solution)/shard_map/ppermute | solution.py:465
  108.8 33.3 %all_to_all.15 = bf16[4,40,2048]{2,1,0:T(8,128)(2,1)S(1)} all-to-all(bf16[4,40,2048]{2,1,0:T(8,128)(2,1)S(1)} %add_convert_fusion), channel_id=1, replica_groups=mesh['z'=8,'yh'=2,'yl'=4,'x'=4,'core'=2] {'x'}, dimensions={0} | all-to-all | bytes 1310720 | tf_op jit(solution)/shard_map/all_to_all | solution.py:467
  142.1 0.8 reduce_sum.12
  (11 shorter events, 0.8 us)
Async XLA Ops:
  11.5 12.2 %collective-permute-start = (bf16[4,320,256]{2,1,0:T(8,128)(2,1)S(1)}, bf16[4,320,256]{2,1,0:T(8,128)(2,1)S(1)}, u32[]{:S(2)}, u32[]{:S(2)}) collective-permute-start(bf16[4,320,256]{2,1,0:T(8,128)(2,1)S(1)} %bitcast.9), channel_id=1, source_target_pairs={{0,1},{1,0},{2,3},{3,2},{4,5},{5,4},{6,7},{7,6},{8,9},{9,8},{10,11... | collective-permute-start | bytes 1966088 | tf_op jit(solution)/shard_map/ppermute | solution.py:369
  30.5 30.8 %all-to-all-start = ((bf16[8,320,128]{2,1,0:T(8,128)(2,1)}), bf16[8,320,128]{2,1,0:T(8,128)(2,1)S(1)}, u32[]{:S(2)}, u32[]{:S(2)}) async-start(bf16[8,320,128]{2,1,0:T(8,128)(2,1)} %get-tuple-element.19), calls=%async_computation | async-start | bytes 1310720 | tf_op jit(solution)/shard_map/all_to_all | solution.py:405
  35.5 9.3 %collective-permute-start.1 = (bf16[320,128]{1,0:T(8,128)(2,1)S(1)}, bf16[320,128]{1,0:T(8,128)(2,1)S(1)}, u32[]{:S(2)}, u32[]{:S(2)}) collective-permute-start(bf16[320,128]{1,0:T(8,128)(2,1)S(1)} %get-tuple-element.20), channel_id=1, source_target_pairs={{0,32},{32,0},{1,33},{33,1},{2,34},{34,2},{3,35},{35,3},{4,36},{36... | collective-permute-start | bytes 245768 | tf_op jit(solution)/shard_map/ppermute | solution.py:387
  73.3 25.5 %all-to-all-start.1 = ((bf16[8,344,128]{2,1,0:T(8,128)(2,1)}), bf16[8,344,128]{2,1,0:T(8,128)(2,1)S(1)}, u32[]{:S(2)}, u32[]{:S(2)}) async-start(bf16[8,344,128]{2,1,0:T(8,128)(2,1)} %shard_map.165), calls=%async_computation.1 | async-start | bytes 1409024 | tf_op jit(solution)/shard_map/all_to_all | solution.py:436
  79.7 5.6 %collective-permute-start.2 = (bf16[128,128]{1,0:T(8,128)(2,1)S(1)}, bf16[128,128]{1,0:T(8,128)(2,1)S(1)}, u32[]{:S(2)}, u32[]{:S(2)}) collective-permute-start(bf16[128,128]{1,0:T(8,128)(2,1)S(1)} %get-tuple-element.26), channel_id=1, source_target_pairs={{0,8},{8,16},{16,24},{24,32},{32,40},{40,48},{48,56},{56,64},{64,7... | collective-permute-start | bytes 98312 | tf_op jit(solution)/shard_map/ppermute | solution.py:410
  81.2 17.6 %copy-start = (bf16[128,2048]{1,0:T(8,128)(2,1)S(1)}, bf16[128,2048]{1,0:T(8,128)(2,1)}, u32[]{:S(2)}) copy-start(bf16[128,2048]{1,0:T(8,128)(2,1)} %wa_ref.3) | copy-start | bytes 1572868
  81.2 17.6 %copy-start.1 = (bf16[128,2048]{1,0:T(8,128)(2,1)S(1)}, bf16[128,2048]{1,0:T(8,128)(2,1)}, u32[]{:S(2)}) copy-start(bf16[128,2048]{1,0:T(8,128)(2,1)} %wb_ref.3) | copy-start | bytes 1572868
  81.2 4.8 %collective-permute-start.3 = (bf16[128,128]{1,0:T(8,128)(2,1)S(1)}, bf16[128,128]{1,0:T(8,128)(2,1)S(1)}, u32[]{:S(2)}, u32[]{:S(2)}) collective-permute-start(bf16[128,128]{1,0:T(8,128)(2,1)S(1)} %get-tuple-element.27), channel_id=1, source_target_pairs={{8,0},{16,8},{24,16},{32,24},{40,32},{48,40},{56,48},{64,56},{72,6... | collective-permute-start | bytes 98312 | tf_op jit(solution)/shard_map/ppermute | solution.py:411
  82.6 1.0 copy-start.2
  83.7 1.0 copy-start.3
  101.0 7.6 %collective-permute-start.4 = (bf16[4,40,2048]{2,1,0:T(8,128)(2,1)S(1)}, bf16[4,40,2048]{2,1,0:T(8,128)(2,1)S(1)}, u32[]{:S(2)}, u32[]{:S(2)}) collective-permute-start(bf16[4,40,2048]{2,1,0:T(8,128)(2,1)S(1)} %get-tuple-element.30), channel_id=1, source_target_pairs={{0,1},{1,0},{2,3},{3,2},{4,5},{5,4},{6,7},{7,6},{8,9},{9,8},{10,11... | collective-permute-start | bytes 1966088 | tf_op jit(solution)/shard_map/ppermute | solution.py:465

commit v3 on v1

--- a/solution.py
+++ b/solution.py
@@ -119,15 +119,15 @@
     rs_low = lax.rsqrt(sum_low / HEAD + EPSILON)
     rs_high = lax.rsqrt(sum_high / HEAD + EPSILON)
     qgain = jnp.concatenate([qgain_ref[0:1, :], qgain_ref[1:2, :]], axis=1)
-    qa = turned(v * jnp.where(low, rs_low, rs_high) * qgain).astype(BF16)
-    for i in range(q_out.shape[0]):
-        q_out[i] = qa
+    q_out[...] = turned(v * jnp.where(low, rs_low, rs_high) * qgain).astype(BF16)
     kv = both_kv[:, :LANES].astype(BF16).astype(F32)
     k_only = jnp.where(low, kv, 0.0)
     sq = jnp.sum(k_only * k_only, axis=1, keepdims=True)
     kgain = jnp.concatenate([kgain_ref[...], kgain_ref[...]], axis=1)
     ka = turned(k_only * lax.rsqrt(sq / HEAD + EPSILON) * kgain)
-    kv_out[...] = jnp.where(low, ka, kv).astype(BF16)
+    both = jnp.where(low, ka, kv).astype(BF16)
+    for i in range(kv_out.shape[0]):
+        kv_out[i] = both
 
 
 def gate_kernel(h_ref, wa_ref, wb_ref, ga_out, gb_out):
@@ -351,10 +351,10 @@
 
     mine = lax.all_gather(tokens, "x", axis=0)
     other = lax.ppermute(mine, "core", [(0, 1), (1, 0)])
-    q8, kv, qb, kvb, kvb_first, kvb_last, normed = call(
+    q, kv8, qb, kvb, kvb_first, kvb_last, normed = call(
         project_kernel,
         (
-            shaped(n_z, rows, LANES), shaped(rows, LANES),
+            shaped(rows, LANES), shaped(n_z, rows, LANES),
             shaped(rows, LANES), shaped(rows, LANES),
             shaped(WINDOW, LANES), shaped(WINDOW, LANES),
             shaped(rows, tp * width),
@@ -373,20 +373,20 @@
         w_qa, w_ka.T, w_va.T, w_qb, w_kb.T, w_vb.T,
         name="project", flops=2 * rows * width * tp * 512, far=set(range(7, 14)),
     )
-    q_all = lax.all_to_all(q8, "z", 0, 0, tiled=True)
-    kv_all = lax.all_gather(kv, "y", axis=0, tiled=True)
+    kv_all = lax.all_to_all(kv8, "z", 0, 0, tiled=True)
+    q_all = lax.all_gather(q, "y", axis=0, tiled=True)
     up = [(i, i + 1) for i in range(blocks - 1)]
     down = [(i + 1, i) for i in range(blocks - 1)]
     before = lax.ppermute(kvb_last, ("z", "y"), up)
     after = lax.ppermute(kvb_first, ("z", "y"), down)
-    n_q = n_z * rows
-    n_k = n_y * rows
+    n_q = n_y * rows
+    n_k = n_z * rows
     tile = 512
     chunk = 256
     steps = 2 * n_q // tile
     parts = call(
         functools.partial(attend_kernel, tile=tile, chunk=chunk),
-        shaped(n_z, rows + STAT_ROWS, LANES),
+        shaped(n_y, rows + STAT_ROWS, LANES),
         [
             pltpu.VMEM((n_k, LANES), BF16),
             pltpu.VMEM((n_k // chunk, HEAD, chunk), BF16),
@@ -399,11 +399,11 @@
         ],
         {},
         {0, 1},
-        q_all.reshape(n_q, LANES), kv_all,
+        q_all, kv_all.reshape(n_k, LANES),
         name="attend", flops=4 * 2 * n_q * n_k * 64,
     )
     parts, normed = lax.optimization_barrier((parts, normed))
-    back = lax.all_to_all(parts, "z", 0, 0, tiled=True)
+    back = lax.all_to_all(parts, "y", 0, 0, tiled=True)
     ga, gb = call(
         gate_kernel,
         (shaped(rows, LANES, dtype=F32), shaped(rows, LANES, dtype=F32)),

time: 139 us -> 131 us (0.942)
  blocking collectives: 68.6 us -> 62.1 us
  waiting for transfers between devices: 11 us -> 9.47 us
    all_to_all x1, blocking collectives: 35 us -> 28.5 us  [body(): arrived = lax.all_to_all(paired, 'x', 0, 0, tiled=True)]
    all_to_all x2, waiting for transfers between devices: 6.59 us -> 1.48 us  [the longest x1 1.48 us: body(): back = lax.all_to_all(parts, 'y', 0, 0, tiled=True)]
    ppermute x1, waiting for transfers between devices: 1.67 us -> 4.88 us  [body(): after = lax.ppermute(kvb_first, ('z', 'y'), down)]
  transfers between devices with their start and end apart: 6 -> 6, of which waited for: 4 -> 5; matrix products, arithmetic and copies ran while one was open for 0% -> 0% of each run, Pallas kernels for 2% -> 2%
where the time goes in v3:
time: 131 us
  blocking collectives  62.1 us (47%)
  starting transfers between devices  34.6 us (26%)
  Pallas kernels  21.1 us (16%)
  waiting for transfers between devices  9.47 us (7%)
  local copies, waits for them, and re-layouts  2.09 us (2%)
  other arithmetic  1.6 us (1%)
    all_to_all x1, blocking collectives, body(): arrived = lax.all_to_all(paired, 'x', 0, 0, tiled=True)  28.5 us
    all_gather x1, blocking collectives, body(): q_all = lax.all_gather(q, 'y', axis=0, tiled=True)  22.1 us
    pallas_call x5, Pallas kernels, call(): pl.pallas_call(kernel, out_shape=outs, in_specs=specs, out_specs=tuple((p...  21.1 us
    all_gather x1, blocking collectives, body(): mine = lax.all_gather(tokens, 'x', axis=0)  11.5 us
    ppermute x1, starting transfers between devices, body(): other = lax.ppermute(mine, 'core', [(0, 1), (1, 0)])  10.5 us
    ppermute x1, starting transfers between devices, body(): got = lax.ppermute(sent, 'core', [(0, 1), (1, 0)])  8.72 us
    all_to_all x1, starting transfers between devices, body(): back = lax.all_to_all(parts, 'y', 0, 0, tiled=True)  5.64 us
    all_to_all x1, starting transfers between devices, body(): kv_all = lax.all_to_all(kv8, 'z', 0, 0, tiled=True)  5.05 us
  transfers between devices with their start and end apart: 6, of which 5 were waited for; matrix products, arithmetic and copies ran while one was open for 0% of the time, Pallas kernels for 2%

profile of v3, /device:TPU:1, one launch (start us, length us, event | category | flops | bytes accessed | tf_op | source)
XLA Modules:
  0.0 131.1 jit_solution(5273755623679142381)
XLA Ops:
  0.0 11.5 %all-gather = bf16[1280,256]{1,0:T(8,128)(2,1)S(1)} all-gather(bf16[320,256]{1,0:T(8,128)(2,1)} %param.17), channel_id=2, replica_groups=mesh['z'=8,'y'=8,'x'=4,'core'=2] {'x'}, dimensions={0}, use_global_device_ids=true | all-gather | bytes 819200 | tf_op jit(solution)/shard_map/all_gather | solution.py:352
  11.5 10.5 %collective-permute-start = (bf16[4,320,256]{2,1,0:T(8,128)(2,1)S(1)}, bf16[4,320,256]{2,1,0:T(8,128)(2,1)S(1)}, u32[]{:S(2)}, u32[]{:S(2)}) collective-permute-start(bf16[4,320,256]{2,1,0:T(8,128)(2,1)S(1)} %bitcast.9), channel_id=1, source_target_pairs={{0,1},{1,0},{2,3},{3,2},{4,5},{5,4},{6,7},{7,6},{8,9},{9,8},{10,11... | collective-permute-start | bytes 1966088 | tf_op jit(solution)/shard_map/ppermute | solution.py:353
  22.0 0.6 pad_add_fusion.place_ref
  22.6 1.1 collective-permute-done.other_ref
  23.7 4.6 %project.1 = (bf16[320,128]{1,0:T(8,128)(2,1)S(1)}, bf16[8,320,128]{2,1,0:T(8,128)(2,1)}, bf16[320,128]{1,0:T(8,128)(2,1)S(1)}, bf16[320,128]{1,0:T(8,128)(2,1)S...) custom-call(s32[2]{0:T(128)} %pad_add_fusion.place_ref, ...), custom_call_target="tpu_custom_call" | custom-call | flops 671088640 | bytes 1048576 | tf_op jit(solution)/shard_map/project/pallas_call | solution.py:319
  28.3 5.0 %all-to-all-start = ((bf16[8,320,128]{2,1,0:T(8,128)(2,1)}), bf16[8,320,128]{2,1,0:T(8,128)(2,1)S(1)}, u32[]{:S(2)}, u32[]{:S(2)}) async-start(bf16[8,320,128]{2,1,0:T(8,128)(2,1)} %get-tuple-element.19), calls=%async_computation | async-start | bytes 1310720 | tf_op jit(solution)/shard_map/all_to_all | solution.py:376
  33.4 22.1 %all_gather.11.q_ref = bf16[2560,128]{1,0:T(8,128)(2,1)S(1)} all-gather(bf16[320,128]{1,0:T(8,128)(2,1)S(1)} %get-tuple-element.18), channel_id=1, replica_groups=mesh['z'=8,'y'=8,'x'=4,'core'=2] {'y'}, dimensions={0}, use_global_device_ids=true | all-gather | bytes 737280 | tf_op jit(solution)/shard_map/all_gather | solution.py:377
  55.4 12.0 %attend.1 = bf16[8,344,128]{2,1,0:T(8,128)(2,1)} custom-call(bf16[2560,128]{1,0:T(8,128)(2,1)S(1)} %all_gather.11.q_ref, bf16[2560,128]{1,0:T(8,128)(2,1)S(1)} %bitcast.11), custom_call_target="tpu_custom_call" | custom-call | flops 3355443200 | bytes 1048576 | tf_op jit(solution)/shard_map/attend/pallas_call | solution.py:319
  67.4 5.6 %all-to-all-start.1 = ((bf16[8,344,128]{2,1,0:T(8,128)(2,1)}), bf16[8,344,128]{2,1,0:T(8,128)(2,1)S(1)}, u32[]{:S(2)}, u32[]{:S(2)}) async-start(bf16[8,344,128]{2,1,0:T(8,128)(2,1)} %attend.1), calls=%async_computation.1 | async-start | bytes 1409024 | tf_op jit(solution)/shard_map/all_to_all | solution.py:406
  73.1 3.4 %collective-permute-start.1 = (bf16[128,128]{1,0:T(8,128)(2,1)S(1)}, bf16[128,128]{1,0:T(8,128)(2,1)S(1)}, u32[]{:S(2)}, u32[]{:S(2)}) collective-permute-start(bf16[128,128]{1,0:T(8,128)(2,1)S(1)} %get-tuple-element.26), channel_id=1, source_target_pairs={{0,8},{8,16},{16,24},{24,32},{32,40},{40,48},{48,56},{56,64},{64,7... | collective-permute-start | bytes 98312 | tf_op jit(solution)/shard_map/ppermute | solution.py:380
  76.5 1.4 %collective-permute-start.2 = (bf16[128,128]{1,0:T(8,128)(2,1)S(1)}, bf16[128,128]{1,0:T(8,128)(2,1)S(1)}, u32[]{:S(2)}, u32[]{:S(2)}) collective-permute-start(bf16[128,128]{1,0:T(8,128)(2,1)S(1)} %get-tuple-element.27), channel_id=1, source_target_pairs={{8,0},{16,8},{24,16},{32,24},{40,32},{48,40},{56,48},{64,56},{72,6... | collective-permute-start | bytes 98312 | tf_op jit(solution)/shard_map/ppermute | solution.py:381
  77.9 1.0 copy-done.2
  78.9 1.0 copy-done.3
  80.0 0.5 gates.1
  80.5 0.3 collective-permute-done.1.prev_ref
  80.8 4.9 %collective-permute-done.2.next_ref = bf16[128,128]{1,0:T(8,128)(2,1)S(1)} collective-permute-done((bf16[128,128]{1,0:T(8,128)(2,1)S(1)}, bf16[128,128]{1,0:T(8,128)(2,1)S(1)}, u32[]{:S(2)}, u32[]{:S(2)}) %collective-permute-start.2) | collective-permute-done | bytes 32800 | tf_op jit(solution)/shard_map/ppermute | solution.py:381
  85.7 1.8 %windowed.1.gated_b_ref = bf16[320,128]{1,0:T(8,128)(2,1)S(1)} custom-call(s32[2]{0:T(128)} %pad_add_fusion.place_ref, bf16[320,128]{1,0:T(8,128)(2,1)S(1)} %get-tuple-element.24.q_ref, bf16[320,128]{1,0:T(8,128)(2,1)S(1)} %get-tuple-element.25.mid_ref, bf16[128,128]{1,0:T(8,128)(2,1)S(1)} %collective-permute-done.1.prev_ref, ...), custom_call_target="tpu_custom_call" | custom-call | flops 94371840 | bytes 1048576 | tf_op jit(solution)/shard_map/windowed/pallas_call | solution.py:319
  87.5 1.5 %all-to-all-done.1.part_ref = bf16[8,344,128]{2,1,0:T(8,128)(2,1)S(1)} async-done(((bf16[8,344,128]{2,1,0:T(8,128)(2,1)}), bf16[8,344,128]{2,1,0:T(8,128)(2,1)S(1)}, u32[]{:S(2)}, u32[]{:S(2)}) %all-to-all-start.1) | async-done | bytes 704544 | tf_op jit(solution)/shard_map/all_to_all | solution.py:406
  89.0 2.2 %combine.1 = (bf16[4,40,2048]{2,1,0:T(8,128)(2,1)S(1)}, bf16[4,40,2048]{2,1,0:T(8,128)(2,1)S(1)}) custom-call(s32[2]{0:T(128)} %pad_add_fusion.place_ref, bf16[8,344,128]{2,1,0:T(8,128)(2,1)S(1)} %all-to-all-done.1.part_ref, f32[320,128]{1,0:T(8,128)S(1)} %get-tuple-element.23.ga_ref, bf16[320,128]{1,0:T(8,128)(2,1)S(1)} %windowed.1.gated_b_ref, ...), custom_call_target="tpu_custom_call" | custom-call | flops 335544320 | bytes 1048576 | tf_op jit(solution)/shard_map/combine/pallas_call | solution.py:319
  91.2 8.7 %collective-permute-start.3 = (bf16[4,40,2048]{2,1,0:T(8,128)(2,1)S(1)}, bf16[4,40,2048]{2,1,0:T(8,128)(2,1)S(1)}, u32[]{:S(2)}, u32[]{:S(2)}) collective-permute-start(bf16[4,40,2048]{2,1,0:T(8,128)(2,1)S(1)} %get-tuple-element.30), channel_id=1, source_target_pairs={{0,1},{1,0},{2,3},{3,2},{4,5},{5,4},{6,7},{7,6},{8,9},{9,8},{10,11... | collective-permute-start | bytes 1966088 | tf_op jit(solution)/shard_map/ppermute | solution.py:435
  99.9 1.7 %collective-permute-done.3 = bf16[4,40,2048]{2,1,0:T(8,128)(2,1)S(1)} collective-permute-done((bf16[4,40,2048]{2,1,0:T(8,128)(2,1)S(1)}, bf16[4,40,2048]{2,1,0:T(8,128)(2,1)S(1)}, u32[]{:S(2)}, u32[]{:S(2)}) %collective-permute-start.3) | collective-permute-done | bytes 655392 | tf_op jit(solution)/shard_map/ppermute | solution.py:435
  101.6 0.2 add_convert_fusion
  101.8 28.5 %all_to_all.15 = bf16[4,40,2048]{2,1,0:T(8,128)(2,1)S(1)} all-to-all(bf16[4,40,2048]{2,1,0:T(8,128)(2,1)S(1)} %add_convert_fusion), channel_id=1, replica_groups=mesh['z'=8,'y'=8,'x'=4,'core'=2] {'x'}, dimensions={0} | all-to-all | bytes 1310720 | tf_op jit(solution)/shard_map/all_to_all | solution.py:437
  130.4 0.8 reduce_sum.12
  (7 shorter events, 0.0 us)
Async XLA Ops:
  11.5 12.2 %collective-permute-start = (bf16[4,320,256]{2,1,0:T(8,128)(2,1)S(1)}, bf16[4,320,256]{2,1,0:T(8,128)(2,1)S(1)}, u32[]{:S(2)}, u32[]{:S(2)}) collective-permute-start(bf16[4,320,256]{2,1,0:T(8,128)(2,1)S(1)} %bitcast.9), channel_id=1, source_target_pairs={{0,1},{1,0},{2,3},{3,2},{4,5},{5,4},{6,7},{7,6},{8,9},{9,8},{10,11... | collective-permute-start | bytes 1966088 | tf_op jit(solution)/shard_map/ppermute | solution.py:353
  28.3 27.1 %all-to-all-start = ((bf16[8,320,128]{2,1,0:T(8,128)(2,1)}), bf16[8,320,128]{2,1,0:T(8,128)(2,1)S(1)}, u32[]{:S(2)}, u32[]{:S(2)}) async-start(bf16[8,320,128]{2,1,0:T(8,128)(2,1)} %get-tuple-element.19), calls=%async_computation | async-start | bytes 1310720 | tf_op jit(solution)/shard_map/all_to_all | solution.py:376
  67.4 21.5 %all-to-all-start.1 = ((bf16[8,344,128]{2,1,0:T(8,128)(2,1)}), bf16[8,344,128]{2,1,0:T(8,128)(2,1)S(1)}, u32[]{:S(2)}, u32[]{:S(2)}) async-start(bf16[8,344,128]{2,1,0:T(8,128)(2,1)} %attend.1), calls=%async_computation.1 | async-start | bytes 1409024 | tf_op jit(solution)/shard_map/all_to_all | solution.py:406
  73.1 7.8 %collective-permute-start.1 = (bf16[128,128]{1,0:T(8,128)(2,1)S(1)}, bf16[128,128]{1,0:T(8,128)(2,1)S(1)}, u32[]{:S(2)}, u32[]{:S(2)}) collective-permute-start(bf16[128,128]{1,0:T(8,128)(2,1)S(1)} %get-tuple-element.26), channel_id=1, source_target_pairs={{0,8},{8,16},{16,24},{24,32},{32,40},{40,48},{48,56},{56,64},{64,7... | collective-permute-start | bytes 98312 | tf_op jit(solution)/shard_map/ppermute | solution.py:380
  76.4 12.5 %copy-start = (bf16[128,2048]{1,0:T(8,128)(2,1)S(1)}, bf16[128,2048]{1,0:T(8,128)(2,1)}, u32[]{:S(2)}) copy-start(bf16[128,2048]{1,0:T(8,128)(2,1)} %wa_ref.3) | copy-start | bytes 1572868
  76.5 12.5 %copy-start.1 = (bf16[128,2048]{1,0:T(8,128)(2,1)S(1)}, bf16[128,2048]{1,0:T(8,128)(2,1)}, u32[]{:S(2)}) copy-start(bf16[128,2048]{1,0:T(8,128)(2,1)} %wb_ref.3) | copy-start | bytes 1572868
  76.5 9.3 %collective-permute-start.2 = (bf16[128,128]{1,0:T(8,128)(2,1)S(1)}, bf16[128,128]{1,0:T(8,128)(2,1)S(1)}, u32[]{:S(2)}, u32[]{:S(2)}) collective-permute-start(bf16[128,128]{1,0:T(8,128)(2,1)S(1)} %get-tuple-element.27), channel_id=1, source_target_pairs={{8,0},{16,8},{24,16},{32,24},{40,32},{48,40},{56,48},{64,56},{72,6... | collective-permute-start | bytes 98312 | tf_op jit(solution)/shard_map/ppermute | solution.py:381
  77.9 1.0 copy-start.2
  78.9 1.0 copy-start.3
  91.2 10.4 %collective-permute-start.3 = (bf16[4,40,2048]{2,1,0:T(8,128)(2,1)S(1)}, bf16[4,40,2048]{2,1,0:T(8,128)(2,1)S(1)}, u32[]{:S(2)}, u32[]{:S(2)}) collective-permute-start(bf16[4,40,2048]{2,1,0:T(8,128)(2,1)S(1)} %get-tuple-element.30), channel_id=1, source_target_pairs={{0,1},{1,0},{2,3},{3,2},{4,5},{5,4},{6,7},{7,6},{8,9},{9,8},{10,11... | collective-permute-start | bytes 1966088 | tf_op jit(solution)/shard_map/ppermute | solution.py:435
